TPU v7x, 32 devices: a whole 2x2x4 slice. The times are simulated.
32 devices in a mesh: sp: 4 (over y, x), tp: 8 (over z, core).
Axes of the slice: x: 2, y: 2, z: 4, core: 2. Of those that a mesh axis runs over, the one named last changes fastest.
Arguments:
- pool_input: bfloat16 [16384, 512], P('sp', 'tp'), may hold values from -6 to 6
- gate_pre: bfloat16 [16384, 1024], P(('sp', 'tp')), may hold values from -8 to 8
- resid: bfloat16 [16384, 1024], P(('sp', 'tp')), may hold values from -6 to 6
- docs: int32 [16384], P('sp'), may hold values from 0 to 3, never falling along the last dimension, each value on 1 to 8192 neighbouring positions
- w_up: bfloat16 [512, 1024], replicated, may hold values from -0.25 to 0.25
- w_out: bfloat16 [1024, 1024], replicated, may hold values from -0.1875 to 0.1875
- g_ffn: float32 [1024], replicated, may hold values from 0.1 to 1.9
- w_gate: bfloat16 [4, 1024, 1024], P('sp'), may hold values from -0.5 to 0.5
- w_lift: bfloat16 [4, 1024, 1024], P('sp'), may hold values from -0.5 to 0.5
- w_down: bfloat16 [4, 1024, 1024], P('sp'), may hold values from -0.0390625 to 0.0390625
- routes: int32 [16384, 2], P(('sp', 'tp')), may hold values from 0 to 3, all different within a row; in each aligned block of 512 rows (0 to 511, 512 to 1023, ...) at most 320 rows name the same one
- route_weight: float32 [16384, 2], P(('sp', 'tp')), may hold values from 0.2 to 1
Outputs:
- layer_out: bfloat16 [16384, 1024], P(('sp', 'tp'))
Inputs may be any that keep to these rules, and one draw needn't show every extreme that they name: `routes`: each row names 2 different experts; among the 512 rows of one device no expert is named more than 320 times. `docs`: document numbers never fall along the sequence.
All inputs are finite; a program needn't handle non-finite values.
Results may differ from a plain program's by a relative error of at most 0.0075.
Values may be sent and summed in bfloat16 or wider, within the bound.
A program may use at most 128 MiB of HBM per device.

v0:
```python
import functools

import jax
import jax.numpy as jnp
from jax import lax
from jax.experimental import pallas as pl
from jax.experimental.pallas import tpu as pltpu
from jax.sharding import PartitionSpec as P

POOL_W = 512
RIM = 15
TILE = 256
LANES = 128
END_SHARE = 6
MESH = pl.DeviceIdType.MESH


def shifted_2(value, axis, steps):
    count = lax.axis_size(axis)
    leading, last = (max(0, -steps), min(count, count - steps))
    return lax.ppermute(value, axis, [(source, source + steps) for source in range(leading, last)])


def partner(me, step, count):
    other, bit = 0, 1
    while bit < count:
        other = other + ((me // bit + step // bit) % 2) * bit
        bit *= 2
    return other


def tile_of(t):
    return pl.ds(pl.multiple_of(t * TILE, TILE), TILE)


def experts_kernel(
    count,
    mixed_ref,
    gain_ref,
    rank_rows_ref,
    rank_cols_ref,
    weight_ref,
    w_gate_hbm,
    w_lift_hbm,
    w_down_hbm,
    out_ref,
    normed,
    onehot,
    send,
    recv,
    result,
    back,
    total,
    act,
    w_gate,
    w_lift,
    w_down,
    weight_sems,
    go_sems,
    come_sems,
    ret_go_sems,
    ret_come_sems,
):
    rows, model_dim = mixed_ref.shape
    cap = send.shape[1]
    hidden = w_gate.shape[1]
    me = lax.axis_index("sp")
    loads = [
        pltpu.make_async_copy(src.at[0], dst, weight_sems.at[i])
        for i, (src, dst) in enumerate(
            ((w_gate_hbm, w_gate), (w_lift_hbm, w_lift), (w_down_hbm, w_down))
        )
    ]

    barrier = pltpu.get_barrier_semaphore()

    def greet(j, carry):
        pl.semaphore_signal(
            barrier, inc=1, device_id={"sp": partner(me, j, count)}, device_id_type=MESH
        )
        return carry

    lax.fori_loop(1, count, greet, 0)
    for load in loads:
        load.start()

    def norm(t, carry):
        block = pl.ds(pl.multiple_of(t * 64, 64), 64)
        x = mixed_ref[block, :].astype(jnp.float32)
        scale = lax.rsqrt(jnp.mean(x * x, axis=-1, keepdims=True) + 1e-06)
        normed[block, :] = (x * scale * gain_ref[...]).astype(jnp.bfloat16)
        return carry

    lax.fori_loop(0, rows // 64, norm, 0)

    def out_copy(j):
        return pltpu.make_async_remote_copy(
            src_ref=send.at[j],
            dst_ref=recv.at[j],
            send_sem=go_sems.at[j],
            recv_sem=come_sems.at[j],
            device_id={"sp": partner(me, j, count)},
            device_id_type=MESH,
        )

    def back_copy(j):
        return pltpu.make_async_remote_copy(
            src_ref=result.at[j],
            dst_ref=back.at[j],
            send_sem=ret_go_sems.at[j],
            recv_sem=ret_come_sems.at[j],
            device_id={"sp": partner(me, j, count)},
            device_id_type=MESH,
        )

    def pack(j, target):
        slot = lax.broadcasted_iota(jnp.int32, (cap, rows), 0)
        onehot[...] = (slot == rank_rows_ref[j]).astype(jnp.float32).astype(jnp.bfloat16)

        def piece(t, carry):
            cols = tile_of(t)
            target[j, :, cols] = jnp.dot(
                onehot[...], normed[:, cols], preferred_element_type=jnp.float32
            ).astype(jnp.bfloat16)
            return carry

        lax.fori_loop(0, model_dim // TILE, piece, 0)

    def ffn(j, source):
        def up(t, carry):
            cols = tile_of(t)
            x = source[j]
            gate = jnp.minimum(jnp.dot(x, w_gate[:, cols], preferred_element_type=jnp.float32), 7.0)
            lift = jnp.clip(
                jnp.dot(x, w_lift[:, cols], preferred_element_type=jnp.float32), -7.0, 7.0
            )
            act[:, cols] = ((lift + 1.0) * gate * jax.nn.sigmoid(1.702 * gate)).astype(jnp.bfloat16)
            return carry

        lax.fori_loop(0, hidden // TILE, up, 0)

        def down(t, carry):
            cols = tile_of(t)
            result[j, :, cols] = jnp.dot(
                act[...], w_down[:, cols], preferred_element_type=jnp.float32
            ).astype(jnp.bfloat16)
            return carry

        lax.fori_loop(0, model_dim // TILE, down, 0)

    def column(ref, j):
        lane = lax.broadcasted_iota(jnp.int32, ref.shape, 1)
        return jnp.sum(jnp.where(lane == j, ref[...], 0.0), axis=1, keepdims=True)

    def combine(j, source, store):
        rank = column(rank_cols_ref, j).astype(jnp.int32)
        weight = column(weight_ref, j)
        slot = lax.broadcasted_iota(jnp.int32, (rows, cap), 1)
        pick = (slot == rank).astype(jnp.float32).astype(jnp.bfloat16)

        def piece(t, carry):
            cols = tile_of(t)
            found = jnp.dot(pick, source[j, :, cols], preferred_element_type=jnp.float32)
            store(cols, weight * found)
            return carry

        lax.fori_loop(0, model_dim // TILE, piece, 0)

    def store_first(cols, term):
        total[:, cols] = mixed_ref[:, cols].astype(jnp.float32) + term

    def store_more(cols, term):
        total[:, cols] = total[:, cols] + term

    def store_last(cols, term):
        out_ref[:, cols] = (total[:, cols] + term).astype(jnp.bfloat16)

    pl.semaphore_wait(barrier, count - 1)

    def dispatch(j, carry):
        pack(j, send)
        out_copy(j).start()
        return carry

    lax.fori_loop(1, count, dispatch, 0)
    pack(0, send)
    for load in loads:
        load.wait()
    ffn(0, send)
    combine(0, result, store_first)

    def serve(j, carry):
        out_copy(j).wait_recv()
        ffn(j, recv)
        back_copy(j).start()
        return carry

    lax.fori_loop(1, count, serve, 0)

    def gather(j, carry):
        back_copy(j).wait_recv()
        combine(j, back, store_more)
        return carry

    lax.fori_loop(1, count - 1, gather, 0)
    back_copy(count - 1).wait_recv()
    combine(count - 1, back, store_last)

    def finish(j, carry):
        out_copy(j).wait_send()
        back_copy(j).wait_send()
        return carry

    lax.fori_loop(1, count, finish, 0)


def run_experts(mixed, gain, rank, weight, w_gate, w_lift, w_down, cap, count):
    rows, model_dim = mixed.shape
    hidden = w_gate.shape[2]
    vmem = pl.BlockSpec(memory_space=pltpu.VMEM)
    anywhere = pl.BlockSpec(memory_space=pl.ANY)
    slots = pltpu.VMEM((count, cap, model_dim), jnp.bfloat16)
    return pl.pallas_call(
        functools.partial(experts_kernel, count),
        out_shape=jax.ShapeDtypeStruct((rows, model_dim), jnp.bfloat16),
        in_specs=[vmem] * 5 + [anywhere] * 3,
        out_specs=vmem,
        scratch_shapes=[
            pltpu.VMEM((rows, model_dim), jnp.bfloat16),
            pltpu.VMEM((cap, rows), jnp.bfloat16),
            slots,
            slots,
            slots,
            slots,
            pltpu.VMEM((rows, model_dim), jnp.float32),
            pltpu.VMEM((cap, hidden), jnp.bfloat16),
            pltpu.VMEM(w_gate.shape[1:], jnp.bfloat16),
            pltpu.VMEM(w_lift.shape[1:], jnp.bfloat16),
            pltpu.VMEM(w_down.shape[1:], jnp.bfloat16),
            pltpu.SemaphoreType.DMA((3,)),
            pltpu.SemaphoreType.DMA((count,)),
            pltpu.SemaphoreType.DMA((count,)),
            pltpu.SemaphoreType.DMA((count,)),
            pltpu.SemaphoreType.DMA((count,)),
        ],
        compiler_params=pltpu.CompilerParams(
            collective_id=0, has_side_effects=True, vmem_limit_bytes=60 * 2**20
        ),
        cost_estimate=pl.CostEstimate(
            flops=6 * count * cap * model_dim * hidden,
            bytes_accessed=3 * model_dim * hidden * 2,
            transcendentals=count * cap * hidden,
        ),
    )(
        mixed,
        gain[None, :],
        rank.T[:, None, :],
        rank.astype(jnp.float32),
        weight,
        w_gate,
        w_lift,
        w_down,
    )


def fused_kernel(
    count,
    tp_count,
    pool_hbm,
    docs_hbm,
    routes_ref,
    route_weight_ref,
    gain_ref,
    gate_hbm,
    resid_hbm,
    w_up_hbm,
    w_out_hbm,
    w_gate_hbm,
    w_lift_hbm,
    w_down_hbm,
    out_ref,
    pool,
    docs,
    gate_pre,
    resid,
    w_up,
    w_out,
    w_gate,
    w_lift,
    w_down,
    pooled,
    gathered,
    tokens,
    gated,
    mixed,
    normed,
    onehot,
    pick_near,
    pick_local,
    send,
    recv,
    result,
    back,
    own,
    corner,
    act,
    corner_act,
    corner_up,
    corner_down,
    corner_out,
    local_out,
    total,
    load_sems,
    edge_go,
    edge_come,
    pool_go,
    pool_come,
    part_go,
    part_come,
    share_go,
    out_go,
    out_come,
    ret_go,
    ret_come,
    core_go,
    core_come,
):
    channels = pool_hbm.shape[0]
    rows, model_dim = resid.shape
    hidden = w_gate.shape[1]
    half = hidden // 2
    cap = own.shape[0]
    part = cap // 2
    sp, tp = lax.axis_index("sp"), lax.axis_index("tp")
    plane, core = tp // 2, tp % 2
    planes = tp_count // 2
    at_end = (plane == 0) | (plane == planes - 1)
    inside = (plane > 0) & (plane < planes - 1)
    f32, bf16 = jnp.float32, jnp.bfloat16

    loads = [
        pltpu.make_async_copy(src, dst, load_sems.at[i])
        for i, (src, dst) in enumerate(
            (
                (pool_hbm, pool.at[:, LANES:]),
                (docs_hbm, docs.at[:, LANES:]),
                (w_up_hbm, w_up),
                (gate_hbm, gate_pre),
                (w_out_hbm, w_out),
                (resid_hbm, resid),
                (w_gate_hbm.at[0], w_gate),
                (w_lift_hbm.at[0], w_lift),
                (w_down_hbm.at[0], w_down),
            )
        )
    ]
    for load in loads[:2]:
        load.start()
    barrier = pltpu.get_barrier_semaphore()

    def greet_sp(j, carry):
        pl.semaphore_signal(
            barrier, inc=1, device_id={"sp": partner(sp, j, count)}, device_id_type=MESH
        )
        return carry

    def greet_tp(j, carry):
        pl.semaphore_signal(
            barrier, inc=1, device_id={"tp": partner(tp, j, tp_count)}, device_id_type=MESH
        )
        return carry

    lax.fori_loop(1, count, greet_sp, 0)
    lax.fori_loop(1, tp_count, greet_tp, 0)
    for load in loads[2:]:
        load.start()

    def remote(src, dst, go, come, device):
        return pltpu.make_async_remote_copy(
            src_ref=src,
            dst_ref=dst,
            send_sem=go,
            recv_sem=come,
            device_id=device,
            device_id_type=MESH,
        )

    following = {"sp": lax.rem(sp + 1, count)}
    tok_dev = pool_hbm.shape[1]
    edges = [
        remote(
            ref.at[:, pl.ds(tok_dev, LANES)],
            ref.at[:, pl.ds(0, LANES)],
            edge_go.at[i],
            edge_come.at[i],
            following,
        )
        for i, ref in enumerate((pool, docs))
    ]

    parts = [(m, q) for q in range(2) for m in range(2)] + [(2, q) for q in range(2)]
    sources = (w_gate_hbm, w_lift_hbm, w_down_hbm)
    inner = (16 - END_SHARE) // 2

    def span(m, q, zone):
        unit = (model_dim if m < 2 else half) // 16
        if isinstance(zone, int) and zone == 0:
            return q * (END_SHARE * unit // 2), END_SHARE * unit // 2
        start = (END_SHARE + inner * (zone - 1)) * unit + q * (inner * unit // 2)
        return pl.multiple_of(start, 16), inner * unit // 2

    def place(m, start, size):
        if m < 2:
            return corner_up.at[m, pl.ds(start, size), :]
        return corner_down.at[pl.ds(start, size), :]

    def fetch(i, zone):
        m, q = parts[i]
        start, size = span(m, q, zone)
        if m < 2:
            cols = pl.ds(pl.multiple_of(core * half, half), half)
            src = sources[m].at[0, pl.ds(start, size), cols]
        else:
            first = pl.multiple_of(core * half + start, 16)
            src = sources[m].at[0, pl.ds(first, size), :]
        return remote(
            src,
            place(m, start, size),
            part_go.at[i],
            part_come.at[zone, i],
            {"sp": partner(sp, 3, count)},
        )

    def share(i, zone, hop):
        m, q = parts[i]
        start, size = span(m, q, zone)
        return remote(
            place(m, start, size),
            place(m, start, size),
            share_go.at[hop - 1, i],
            part_come.at[zone, i],
            {"tp": partner(tp, 2 * hop, tp_count)},
        )

    def pass_on(i):
        @pl.when(at_end)
        def _():
            fetch(i, 0).wait_recv()
            share(i, 0, 1).start()

        @pl.when(inside)
        def _():
            fetch(i, plane).wait_recv()
            for hop in (3, 2, 1):
                share(i, plane, hop).start()

    def arrived(i):
        @pl.when(at_end)
        def _():
            share(i, 1, 1).wait_recv()
            share(i, 2, 1).wait_recv()

        @pl.when(inside)
        def _():
            share(i, 0, 1).wait_recv()
            share(i, 3 - plane, 1).wait_recv()

    for load in loads[:2]:
        load.wait()
    pl.semaphore_wait(barrier, count - 1 + tp_count - 1)
    for edge in edges:
        edge.start()

    @pl.when(at_end)
    def _():
        for i in range(len(parts)):
            fetch(i, 0).start()

    @pl.when(inside)
    def _():
        for i in range(len(parts)):
            fetch(i, plane).start()

    first, second = routes_ref[0:1, :], routes_ref[1:2, :]
    weight_first, weight_second = route_weight_ref[0:1, :], route_weight_ref[1:2, :]
    named, weights = [], []
    for j in range(count):
        expert = partner(sp, j, count)
        named.append(jnp.where((first == expert) | (second == expert), 1.0, 0.0))
        weights.append(
            jnp.where(first == expert, weight_first, 0.0)
            + jnp.where(second == expert, weight_second, 0.0)
        )
    named = jnp.concatenate(named + named, axis=0)
    weights = jnp.concatenate(weights + weights, axis=0)
    before = lax.broadcasted_iota(jnp.int32, (rows, rows), 0) <= lax.broadcasted_iota(
        jnp.int32, (rows, rows), 1
    )
    place_of = jnp.dot(
        named.astype(bf16), before.astype(f32).astype(bf16), preferred_element_type=f32
    )
    place_of = jnp.where(named > 0.0, place_of - 1.0, -4.0 * cap)
    split = jnp.where(place_of >= part, place_of + part, place_of)
    line = lax.broadcasted_iota(jnp.int32, place_of.shape, 0)
    goal = jnp.where(line == 1, split, place_of)
    goal = jnp.where(line == 2, split + part, goal)
    goal = jnp.where(line == 3, place_of + cap, goal)
    goal_rows = goal.astype(jnp.int32)
    goal_cols = goal.T.astype(jnp.int32)
    weight_cols = weights.T

    slot = lax.broadcasted_iota(jnp.int32, (2 * cap, rows), 0)
    for k, (a, b) in enumerate(((1, 2), (0, 3))):
        hit = (slot == goal_rows[a : a + 1, :]) | (slot == goal_rows[b : b + 1, :])
        onehot[k] = hit.astype(f32).astype(bf16)

    def weighed(slots, j, shift):
        return jnp.where(
            slots == goal_cols[:, j : j + 1] + shift, weight_cols[:, j : j + 1], 0.0
        )

    near_slots = lax.broadcasted_iota(jnp.int32, (rows, 2 * cap), 1)
    pick_near[...] = (weighed(near_slots, 1, 0) + weighed(near_slots, 2, 0)).astype(bf16)
    local_slots = lax.broadcasted_iota(jnp.int32, (rows, 3 * cap), 1)
    pick_local[...] = (
        weighed(local_slots, 0, 0) + weighed(local_slots, 3, 0) + weighed(local_slots, 3, cap)
    ).astype(bf16)

    level = (tp * channels) // (channels * tp_count // 4)
    for edge in edges:
        edge.wait_recv()

    def pool_copy(j):
        return remote(
            pooled.at[j],
            gathered.at[pl.ds(pl.multiple_of(tp * channels, channels), channels), :],
            pool_go.at[j],
            pool_come.at[j],
            {"tp": partner(tp, j, tp_count)},
        )

    def pool_block(j):
        owner = partner(tp, j, tp_count)
        cols = pl.ds(pl.multiple_of(owner * rows, LANES), rows + LANES)
        values = pool[:, cols].astype(f32)
        document = jnp.broadcast_to(docs[:, cols], (8, rows + LANES))
        lane = lax.broadcasted_iota(jnp.int32, document.shape, 1)
        document = jnp.where((lane < LANES) & (owner == 0) & (sp == 0), -1, document)
        running = values
        number = jnp.ones(document.shape, f32)
        for step in range(4):
            shift = 2**step
            same = (document == pltpu.roll(document, shift, 1)) & (level >= step)
            same = same.astype(f32)
            number = number + same * pltpu.roll(number, shift, 1)
            wide = jnp.concatenate([same] * (channels // 8), axis=0)
            running = running + wide * pltpu.roll(running, shift, 1)
        share_of = jnp.concatenate([1.0 / number] * (channels // 8), axis=0)
        return (running * share_of - values)[:, LANES:].astype(bf16)

    def pool_step(i, carry):
        j = tp_count - 1 - i
        pooled[j] = pool_block(j)
        pool_copy(j).start()
        return carry

    lax.fori_loop(0, tp_count - 1, pool_step, 0)
    gathered[pl.ds(pl.multiple_of(tp * channels, channels), channels), :] = pool_block(0)

    for i in range(3):
        pass_on(i)

    for load in loads[2:6]:
        load.wait()

    def pool_wait(j, carry):
        pool_copy(j).wait_recv()
        return carry

    lax.fori_loop(1, tp_count, pool_wait, 0)
    tokens[...] = gathered[...].T

    def lift_up(t, carry):
        cols = tile_of(t)
        lifted = jnp.dot(tokens[...], w_up[:, cols], preferred_element_type=f32)
        gated[:, cols] = (jax.nn.sigmoid(gate_pre[:, cols].astype(f32)) * lifted).astype(bf16)
        return carry

    lax.fori_loop(0, model_dim // TILE, lift_up, 0)

    def mix(t, carry):
        cols = tile_of(t)
        added = jnp.dot(gated[...], w_out[:, cols], preferred_element_type=f32)
        mixed[:, cols] = (resid[:, cols].astype(f32) + added).astype(bf16)
        return carry

    lax.fori_loop(0, model_dim // TILE, mix, 0)

    def norm(t, carry):
        block = pl.ds(pl.multiple_of(t * 64, 64), 64)
        x = mixed[block, :].astype(f32)
        scale = lax.rsqrt(jnp.mean(x * x, axis=-1, keepdims=True) + 1e-06)
        normed[block, :] = (x * scale * gain_ref[...]).astype(bf16)
        return carry

    lax.fori_loop(0, rows // 64, norm, 0)

    def pack_near(t, carry):
        cols = tile_of(t)
        send[:, cols] = jnp.dot(
            onehot[0], normed[:, cols], preferred_element_type=f32
        ).astype(bf16)
        return carry

    lax.fori_loop(0, model_dim // TILE, pack_near, 0)

    def out_copy(h, p):
        block = pl.ds((2 * h + p) * part, part)
        return remote(
            send.at[block],
            recv.at[block],
            out_go.at[2 * h + p],
            out_come.at[2 * h + p],
            {"sp": partner(sp, p + 1, count)},
        )

    def back_copy(h, p):
        block = pl.ds((2 * h + p) * part, part)
        return remote(
            result.at[block],
            back.at[block],
            ret_go.at[2 * h + p],
            ret_come.at[2 * h + p],
            {"sp": partner(sp, p + 1, count)},
        )

    chunks = [(h, p) for h in range(2) for p in range(2)]
    for h, p in chunks:
        out_copy(h, p).start()

    def pack_local(t, carry):
        cols = tile_of(t)
        packed = jnp.dot(onehot[1], normed[:, cols], preferred_element_type=f32).astype(bf16)
        own[:, cols] = packed[:cap]
        corner[0:cap, cols] = packed[cap:]
        return carry

    lax.fori_loop(0, model_dim // TILE, pack_local, 0)
    mate = {"tp": partner(tp, 1, tp_count)}
    corner_copy = remote(
        corner.at[pl.ds(0, cap)], corner.at[pl.ds(cap, cap)], core_go.at[0], core_come.at[0], mate
    )
    corner_copy.start()
    pass_on(3)

    def activate(gate, lift):
        gate = jnp.minimum(gate, 7.0)
        lift = jnp.clip(lift, -7.0, 7.0)
        return ((lift + 1.0) * gate * jax.nn.sigmoid(1.702 * gate)).astype(bf16)

    def ffn(source, target, base):
        def up(t, carry):
            cols = tile_of(t)
            x = source[base : base + cap, :]
            act[:, cols] = activate(
                jnp.dot(x, w_gate[:, cols], preferred_element_type=f32),
                jnp.dot(x, w_lift[:, cols], preferred_element_type=f32),
            )
            return carry

        lax.fori_loop(0, hidden // TILE, up, 0)

        def down(t, carry):
            cols = tile_of(t)
            target[base : base + cap, cols] = jnp.dot(
                act[...], w_down[:, cols], preferred_element_type=f32
            ).astype(bf16)
            return carry

        lax.fori_loop(0, model_dim // TILE, down, 0)

    for load in loads[6:]:
        load.wait()
    ffn(own, local_out, 0)
    pass_on(4)
    pass_on(5)

    for h in range(2):
        for p in range(2):
            out_copy(h, p).wait_recv()
        ffn(recv, result, h * cap)
        for p in range(2):
            back_copy(h, p).start()

    corner_copy.wait_recv()
    for i in range(4):
        arrived(i)

    def corner_lift(t, carry):
        cols = tile_of(t)
        x = corner[...]
        corner_act[:, cols] = activate(
            jnp.dot(x, corner_up[0, :, cols], preferred_element_type=f32),
            jnp.dot(x, corner_up[1, :, cols], preferred_element_type=f32),
        )
        return carry

    lax.fori_loop(0, half // TILE, corner_lift, 0)
    for i in range(4, 6):
        arrived(i)

    def corner_drop(t, carry):
        cols = tile_of(t)
        found = jnp.dot(
            corner_act[...], corner_down[:, cols], preferred_element_type=f32
        ).astype(bf16)
        local_out[cap : 2 * cap, cols] = found[:cap]
        corner_out[:, cols] = found[cap:]
        return carry

    lax.fori_loop(0, model_dim // TILE, corner_drop, 0)
    mate_copy = remote(
        corner_out, local_out.at[pl.ds(2 * cap, cap)], core_go.at[1], core_come.at[1], mate
    )
    mate_copy.start()
    mate_copy.wait_recv()

    def combine_local(t, carry):
        cols = tile_of(t)
        total[:, cols] = mixed[:, cols].astype(f32) + jnp.dot(
            pick_local[...], local_out[:, cols], preferred_element_type=f32
        )
        return carry

    lax.fori_loop(0, model_dim // TILE, combine_local, 0)
    for h, p in chunks:
        back_copy(h, p).wait_recv()

    def combine_near(t, carry):
        cols = tile_of(t)
        found = jnp.dot(pick_near[...], back[:, cols], preferred_element_type=f32)
        out_ref[:, cols] = (total[:, cols] + found).astype(bf16)
        return carry

    lax.fori_loop(0, model_dim // TILE, combine_near, 0)

    for edge in edges:
        edge.wait_send()

    def pool_sent(j, carry):
        pool_copy(j).wait_send()
        return carry

    lax.fori_loop(1, tp_count, pool_sent, 0)
    for h, p in chunks:
        out_copy(h, p).wait_send()
        back_copy(h, p).wait_send()
    corner_copy.wait_send()
    mate_copy.wait_send()
    for i in range(len(parts)):

        @pl.when(at_end)
        def _():
            fetch(i, 0).wait_send()
            share(i, 0, 1).wait_send()

        @pl.when(inside)
        def _():
            fetch(i, plane).wait_send()
            for hop in (1, 2, 3):
                share(i, plane, hop).wait_send()


def run_fused(
    count,
    tp_count,
    pool_input,
    gate_pre,
    resid,
    docs,
    w_up,
    w_out,
    g_ffn,
    w_gate,
    w_lift,
    w_down,
    routes,
    route_weight,
):
    tok_dev, channels = pool_input.shape
    rows, model_dim = resid.shape
    hidden = w_gate.shape[2]
    half = hidden // 2
    pool_w = w_up.shape[0]
    cap = capacity(rows, routes.shape[1], count)
    vmem = pl.BlockSpec(memory_space=pltpu.VMEM)
    anywhere = pl.BlockSpec(memory_space=pl.ANY)
    bf16, f32 = jnp.bfloat16, jnp.float32
    dma = pltpu.SemaphoreType.DMA
    return pl.pallas_call(
        functools.partial(fused_kernel, count, tp_count),
        out_shape=jax.ShapeDtypeStruct((rows, model_dim), bf16),
        in_specs=[anywhere] * 2 + [vmem] * 3 + [anywhere] * 7,
        out_specs=vmem,
        scratch_shapes=[
            pltpu.VMEM((channels, tok_dev + LANES), bf16),
            pltpu.VMEM((1, tok_dev + LANES), jnp.int32),
            pltpu.VMEM((rows, model_dim), bf16),
            pltpu.VMEM((rows, model_dim), bf16),
            pltpu.VMEM(w_up.shape, bf16),
            pltpu.VMEM(w_out.shape, bf16),
            pltpu.VMEM(w_gate.shape[1:], bf16),
            pltpu.VMEM(w_lift.shape[1:], bf16),
            pltpu.VMEM(w_down.shape[1:], bf16),
            pltpu.VMEM((tp_count, channels, rows), bf16),
            pltpu.VMEM((pool_w, rows), bf16),
            pltpu.VMEM((rows, pool_w), bf16),
            pltpu.VMEM((rows, model_dim), bf16),
            pltpu.VMEM((rows, model_dim), bf16),
            pltpu.VMEM((rows, model_dim), bf16),
            pltpu.VMEM((2, 2 * cap, rows), bf16),
            pltpu.VMEM((rows, 2 * cap), bf16),
            pltpu.VMEM((rows, 3 * cap), bf16),
            pltpu.VMEM((2 * cap, model_dim), bf16),
            pltpu.VMEM((2 * cap, model_dim), bf16),
            pltpu.VMEM((2 * cap, model_dim), bf16),
            pltpu.VMEM((2 * cap, model_dim), bf16),
            pltpu.VMEM((cap, model_dim), bf16),
            pltpu.VMEM((2 * cap, model_dim), bf16),
            pltpu.VMEM((cap, hidden), bf16),
            pltpu.VMEM((2 * cap, half), bf16),
            pltpu.VMEM((2, model_dim, half), bf16),
            pltpu.VMEM((half, model_dim), bf16),
            pltpu.VMEM((cap, model_dim), bf16),
            pltpu.VMEM((3 * cap, model_dim), bf16),
            pltpu.VMEM((rows, model_dim), f32),
            dma((9,)),
            dma((2,)),
            dma((2,)),
            dma((tp_count,)),
            dma((tp_count,)),
            dma((6,)),
            dma((3, 6)),
            dma((3, 6)),
            dma((4,)),
            dma((4,)),
            dma((4,)),
            dma((4,)),
            dma((2,)),
            dma((2,)),
        ],
        compiler_params=pltpu.CompilerParams(
            collective_id=1, has_side_effects=True, vmem_limit_bytes=60 * 2**20
        ),
        cost_estimate=pl.CostEstimate(
            flops=6 * count * cap * model_dim * hidden,
            bytes_accessed=3 * model_dim * hidden * 2,
            transcendentals=count * cap * hidden,
        ),
    )(
        pool_input.T,
        docs[None, :],
        routes.T,
        route_weight.T,
        g_ffn[None, :],
        gate_pre,
        resid,
        w_up,
        w_out,
        w_gate,
        w_lift,
        w_down,
    )


def capacity(row_count, top_count, count):
    cap = max(2, 5 * row_count * top_count // (4 * count))
    return (cap + 15) // 16 * 16


def on_device(
    pool_input,
    gate_pre,
    resid,
    docs,
    w_up,
    w_out,
    g_ffn,
    w_gate,
    w_lift,
    w_down,
    routes,
    route_weight,
):
    tok_dev = pool_input.shape[0]
    channels = pool_input.shape[1]
    group_size = POOL_W // 4
    channel_ids = lax.axis_index("tp") * channels + lax.iota(jnp.int32, channels)
    window = jnp.power(2, channel_ids // group_size + 1)
    edge = jnp.concatenate(
        [pool_input[tok_dev - RIM :], docs[tok_dev - RIM :, None].astype(jnp.bfloat16)], axis=1
    )
    before = shifted_2(edge, "sp", 1)
    before_rows = before[:, :channels]
    before_docs = before[:, channels].astype(jnp.int32)
    first_dev = lax.axis_index("sp") == 0
    before_docs = jnp.where(first_dev, -1, before_docs)
    values = pool_input.astype(jnp.float32)
    padded = jnp.concatenate([before_rows.astype(jnp.float32), values], axis=0)
    doc_padded = jnp.concatenate([before_docs.astype(jnp.int32), docs], axis=0)
    earlier = sum(
        (doc_padded[RIM - offset : RIM - offset + tok_dev] == docs).astype(jnp.int32)
        for offset in range(1, RIM + 1)
    )
    reach = jnp.minimum(earlier[:, None] + 1, window[None, :])
    running = values
    for offset in range(1, RIM + 1):
        shifted = padded[RIM - offset : RIM - offset + tok_dev]
        running = running + jnp.where(offset < reach, shifted, 0.0)
    counts = reach.astype(jnp.float32)
    pooled = (running / counts - values).astype(jnp.bfloat16)
    tokens_pooled = lax.all_to_all(pooled, "tp", split_axis=0, concat_axis=1, tiled=True)
    lifted = jnp.dot(tokens_pooled, w_up, preferred_element_type=jnp.float32)
    gated_rows = (jax.nn.sigmoid(gate_pre.astype(jnp.float32)) * lifted).astype(jnp.bfloat16)
    mixed_rows = (
        resid.astype(jnp.float32) + jnp.dot(gated_rows, w_out, preferred_element_type=jnp.float32)
    ).astype(jnp.bfloat16)

    row_count, top_count = routes.shape
    count = lax.axis_size("sp")
    cap = capacity(row_count, top_count, count)
    order = partner(lax.axis_index("sp"), lax.iota(jnp.int32, count), count)
    chosen = routes[:, :, None] == order[None, None, :]
    named = jnp.any(chosen, axis=1)
    rank = jnp.where(named, jnp.cumsum(named.astype(jnp.int32), axis=0) - 1, -1)
    weight = jnp.sum(jnp.where(chosen, route_weight[:, :, None], 0.0), axis=1)
    return run_experts(mixed_rows, g_ffn, rank, weight, w_gate, w_lift, w_down, cap, count)


def solution(mesh):
    in_specs = (
        P("sp", "tp"),
        P(("sp", "tp"), None),
        P(("sp", "tp"), None),
        P("sp"),
        P(),
        P(),
        P(),
        P("sp", None, None),
        P("sp", None, None),
        P("sp", None, None),
        P(("sp", "tp"), None),
        P(("sp", "tp"), None),
    )
    out_specs = P(("sp", "tp"), None)
    count, tp_count = mesh.shape["sp"], mesh.shape["tp"]
    body = on_device
    if count == 4 and tp_count == 8:
        body = functools.partial(run_fused, count, tp_count)
    return jax.shard_map(
        body, mesh=mesh, in_specs=in_specs, out_specs=out_specs, check_vma=False
    )
```

profile of v0, /device:TPU:0, one launch (start us, length us, event | category | flops | bytes accessed | tf_op | source)
XLA Modules:
  0.0 74.6 jit_solution(13713698403103000026)
XLA Ops:
  0.0 72.3 %shard_map.118 = bf16[512,1024]{1,0:T(8,128)(2,1)} custom-call(bf16[64,4096]{1,0:T(8,128)(2,1)} %bitcast.5, s32[1,4096]{1,0:T(1,128)} %bitcast.6, s32[2,512]{1,0:T(2,128)} %bitcast.7, f32[2,512]{1,0:T(2,128)} %bitcast.8, f32[1,1024]{1,0:T(1,128)} %bitcast.9, bf16[512,1024]{1,0:T(8,128)(2,1)} %gate_hbm.1, bf16[512,1024]{1,0:T(8,128)(2,1)} %resid_hbm.1, ...), custom_call_target="tpu_custom_call" | custom-call | flops 8053063680 | bytes 6291456 | tf_op jit(solution)/shard_map/pallas_call | solution.py:800
  72.3 2.3 %copy.14 = bf16[512,1024]{1,0:T(8,128)(2,1)} copy(bf16[512,1024]{1,0:T(8,128)(2,1)} %shard_map.118) | data formatting | bytes 2097152
where the time goes:
time: 75.4 us; the launch traced here: 74.6 us
  Pallas kernels  72.3 us (96%)
  local copies, waits for them, and re-layouts  2.26 us (3%)
    pallas_call x1, Pallas kernels, run_fused(): pl.pallas_call(functools.partial(fused_kernel, count, tp_count), out_shap...  72.3 us
    unnamed x1, local copies, waits for them, and re-layouts  2.26 us

commit v1 on v0

--- a/solution.py
+++ b/solution.py
@@ -268,9 +268,9 @@
     tp_count,
     pool_hbm,
     docs_hbm,
-    routes_ref,
-    route_weight_ref,
-    gain_ref,
+    routes_hbm,
+    route_weight_hbm,
+    gain_hbm,
     gate_hbm,
     resid_hbm,
     w_up_hbm,
@@ -281,6 +281,9 @@
     out_ref,
     pool,
     docs,
+    routes_ref,
+    route_weight_ref,
+    gain,
     gate_pre,
     resid,
     w_up,
@@ -295,8 +298,8 @@
     mixed,
     normed,
     onehot,
-    pick_near,
-    pick_local,
+    pick_own,
+    pick_rest,
     send,
     recv,
     result,
@@ -344,10 +347,13 @@
             (
                 (pool_hbm, pool.at[:, LANES:]),
                 (docs_hbm, docs.at[:, LANES:]),
+                (routes_hbm, routes_ref),
+                (route_weight_hbm, route_weight_ref),
                 (w_up_hbm, w_up),
                 (gate_hbm, gate_pre),
                 (w_out_hbm, w_out),
                 (resid_hbm, resid),
+                (gain_hbm, gain),
                 (w_gate_hbm.at[0], w_gate),
                 (w_lift_hbm.at[0], w_lift),
                 (w_down_hbm.at[0], w_down),
@@ -398,16 +404,16 @@
         for i, ref in enumerate((pool, docs))
     ]
 
-    parts = [(m, q) for q in range(2) for m in range(2)] + [(2, q) for q in range(2)]
+    parts = [(m, q) for q in range(4) for m in range(2)] + [(2, q) for q in range(2)]
     sources = (w_gate_hbm, w_lift_hbm, w_down_hbm)
     inner = (16 - END_SHARE) // 2
 
     def span(m, q, zone):
-        unit = (model_dim if m < 2 else half) // 16
+        unit, cuts = (model_dim // 16, 4) if m < 2 else (half // 16, 2)
         if isinstance(zone, int) and zone == 0:
-            return q * (END_SHARE * unit // 2), END_SHARE * unit // 2
-        start = (END_SHARE + inner * (zone - 1)) * unit + q * (inner * unit // 2)
-        return pl.multiple_of(start, 16), inner * unit // 2
+            return q * (END_SHARE * unit // cuts), END_SHARE * unit // cuts
+        start = (END_SHARE + inner * (zone - 1)) * unit + q * (inner * unit // cuts)
+        return pl.multiple_of(start, 16), inner * unit // cuts
 
     def place(m, start, size):
         if m < 2:
@@ -481,54 +487,7 @@
         for i in range(len(parts)):
             fetch(i, plane).start()
 
-    first, second = routes_ref[0:1, :], routes_ref[1:2, :]
-    weight_first, weight_second = route_weight_ref[0:1, :], route_weight_ref[1:2, :]
-    named, weights = [], []
-    for j in range(count):
-        expert = partner(sp, j, count)
-        named.append(jnp.where((first == expert) | (second == expert), 1.0, 0.0))
-        weights.append(
-            jnp.where(first == expert, weight_first, 0.0)
-            + jnp.where(second == expert, weight_second, 0.0)
-        )
-    named = jnp.concatenate(named + named, axis=0)
-    weights = jnp.concatenate(weights + weights, axis=0)
-    before = lax.broadcasted_iota(jnp.int32, (rows, rows), 0) <= lax.broadcasted_iota(
-        jnp.int32, (rows, rows), 1
-    )
-    place_of = jnp.dot(
-        named.astype(bf16), before.astype(f32).astype(bf16), preferred_element_type=f32
-    )
-    place_of = jnp.where(named > 0.0, place_of - 1.0, -4.0 * cap)
-    split = jnp.where(place_of >= part, place_of + part, place_of)
-    line = lax.broadcasted_iota(jnp.int32, place_of.shape, 0)
-    goal = jnp.where(line == 1, split, place_of)
-    goal = jnp.where(line == 2, split + part, goal)
-    goal = jnp.where(line == 3, place_of + cap, goal)
-    goal_rows = goal.astype(jnp.int32)
-    goal_cols = goal.T.astype(jnp.int32)
-    weight_cols = weights.T
-
-    slot = lax.broadcasted_iota(jnp.int32, (2 * cap, rows), 0)
-    for k, (a, b) in enumerate(((1, 2), (0, 3))):
-        hit = (slot == goal_rows[a : a + 1, :]) | (slot == goal_rows[b : b + 1, :])
-        onehot[k] = hit.astype(f32).astype(bf16)
-
-    def weighed(slots, j, shift):
-        return jnp.where(
-            slots == goal_cols[:, j : j + 1] + shift, weight_cols[:, j : j + 1], 0.0
-        )
-
-    near_slots = lax.broadcasted_iota(jnp.int32, (rows, 2 * cap), 1)
-    pick_near[...] = (weighed(near_slots, 1, 0) + weighed(near_slots, 2, 0)).astype(bf16)
-    local_slots = lax.broadcasted_iota(jnp.int32, (rows, 3 * cap), 1)
-    pick_local[...] = (
-        weighed(local_slots, 0, 0) + weighed(local_slots, 3, 0) + weighed(local_slots, 3, cap)
-    ).astype(bf16)
-
     level = (tp * channels) // (channels * tp_count // 4)
-    for edge in edges:
-        edge.wait_recv()
 
     def pool_copy(j):
         return remote(
@@ -558,19 +517,82 @@
         share_of = jnp.concatenate([1.0 / number] * (channels // 8), axis=0)
         return (running * share_of - values)[:, LANES:].astype(bf16)
 
+    def pool_send(j):
+        pooled[j] = pool_block(j)
+        pool_copy(j).start()
+
     def pool_step(i, carry):
         j = tp_count - 1 - i
-        pooled[j] = pool_block(j)
-        pool_copy(j).start()
+
+        @pl.when(j != tp)
+        def _():
+            pool_send(j)
+
         return carry
 
     lax.fori_loop(0, tp_count - 1, pool_step, 0)
+    for edge in edges:
+        edge.wait_recv()
+
+    @pl.when(tp != 0)
+    def _():
+        pool_send(tp)
+
     gathered[pl.ds(pl.multiple_of(tp * channels, channels), channels), :] = pool_block(0)
-
-    for i in range(3):
+    pass_on(0)
+
+    for load in loads[2:4]:
+        load.wait()
+
+    first, second = routes_ref[0:1, :], routes_ref[1:2, :]
+    weight_first, weight_second = route_weight_ref[0:1, :], route_weight_ref[1:2, :]
+    named, weights = [], []
+    for j in range(count):
+        expert = partner(sp, j, count)
+        named.append(jnp.where((first == expert) | (second == expert), 1.0, 0.0))
+        weights.append(
+            jnp.where(first == expert, weight_first, 0.0)
+            + jnp.where(second == expert, weight_second, 0.0)
+        )
+    named = jnp.concatenate(named + named, axis=0)
+    weights = jnp.concatenate(weights + weights, axis=0)
+    before = lax.broadcasted_iota(jnp.int32, (rows, rows), 0) <= lax.broadcasted_iota(
+        jnp.int32, (rows, rows), 1
+    )
+    place_of = jnp.dot(
+        named.astype(bf16), before.astype(f32).astype(bf16), preferred_element_type=f32
+    )
+    place_of = jnp.where(named > 0.0, place_of - 1.0, -4.0 * cap)
+    split = jnp.where(place_of >= part, place_of + part, place_of)
+    line = lax.broadcasted_iota(jnp.int32, place_of.shape, 0)
+    goal = jnp.where(line == 1, split, place_of)
+    goal = jnp.where(line == 2, split + part, goal)
+    goal = jnp.where(line == 3, place_of + cap, goal)
+    goal_rows = goal.astype(jnp.int32)
+    goal_cols = goal.T.astype(jnp.int32)
+    weight_cols = weights.T
+
+    slot = lax.broadcasted_iota(jnp.int32, (2 * cap, rows), 0)
+    for k, (a, b) in enumerate(((1, 2), (0, 3))):
+        hit = (slot == goal_rows[a : a + 1, :]) | (slot == goal_rows[b : b + 1, :])
+        onehot[k] = hit.astype(f32).astype(bf16)
+
+    def weighed(slots, j, shift):
+        return jnp.where(
+            slots == goal_cols[:, j : j + 1] + shift, weight_cols[:, j : j + 1], 0.0
+        )
+
+    slots = lax.broadcasted_iota(jnp.int32, (rows, cap), 1)
+    pick_own[...] = weighed(slots, 0, 0).astype(bf16)
+    slots = lax.broadcasted_iota(jnp.int32, (rows, 4 * cap), 1)
+    found = weighed(slots, 1, 0) + weighed(slots, 2, 0)
+    found = found + weighed(slots, 3, cap) + weighed(slots, 3, 2 * cap)
+    pick_rest[...] = found.astype(bf16)
+
+    for i in range(1, 4):
         pass_on(i)
 
-    for load in loads[2:6]:
+    for load in loads[4:9]:
         load.wait()
 
     def pool_wait(j, carry):
@@ -600,9 +622,11 @@
         block = pl.ds(pl.multiple_of(t * 64, 64), 64)
         x = mixed[block, :].astype(f32)
         scale = lax.rsqrt(jnp.mean(x * x, axis=-1, keepdims=True) + 1e-06)
-        normed[block, :] = (x * scale * gain_ref[...]).astype(bf16)
-        return carry
-
+        normed[block, :] = (x * scale * gain[...]).astype(bf16)
+        return carry
+
+    for i in range(4, 6):
+        pass_on(i)
     lax.fori_loop(0, rows // 64, norm, 0)
 
     def pack_near(t, carry):
@@ -638,6 +662,8 @@
     for h, p in chunks:
         out_copy(h, p).start()
 
+    pass_on(6)
+
     def pack_local(t, carry):
         cols = tile_of(t)
         packed = jnp.dot(onehot[1], normed[:, cols], preferred_element_type=f32).astype(bf16)
@@ -651,7 +677,7 @@
         corner.at[pl.ds(0, cap)], corner.at[pl.ds(cap, cap)], core_go.at[0], core_come.at[0], mate
     )
     corner_copy.start()
-    pass_on(3)
+    pass_on(7)
 
     def activate(gate, lift):
         gate = jnp.minimum(gate, 7.0)
@@ -679,11 +705,20 @@
 
         lax.fori_loop(0, model_dim // TILE, down, 0)
 
-    for load in loads[6:]:
+    for load in loads[9:]:
         load.wait()
     ffn(own, local_out, 0)
-    pass_on(4)
-    pass_on(5)
+    pass_on(8)
+
+    def combine_own(t, carry):
+        cols = tile_of(t)
+        total[:, cols] = mixed[:, cols].astype(f32) + jnp.dot(
+            pick_own[...], local_out[:, cols], preferred_element_type=f32
+        )
+        return carry
+
+    lax.fori_loop(0, model_dim // TILE, combine_own, 0)
+    pass_on(9)
 
     for h in range(2):
         for p in range(2):
@@ -693,7 +728,7 @@
             back_copy(h, p).start()
 
     corner_copy.wait_recv()
-    for i in range(4):
+    for i in range(8):
         arrived(i)
 
     def corner_lift(t, carry):
@@ -706,43 +741,38 @@
         return carry
 
     lax.fori_loop(0, half // TILE, corner_lift, 0)
-    for i in range(4, 6):
+    for i in range(8, 10):
         arrived(i)
 
-    def corner_drop(t, carry):
-        cols = tile_of(t)
-        found = jnp.dot(
-            corner_act[...], corner_down[:, cols], preferred_element_type=f32
-        ).astype(bf16)
-        local_out[cap : 2 * cap, cols] = found[:cap]
-        corner_out[:, cols] = found[cap:]
-        return carry
-
-    lax.fori_loop(0, model_dim // TILE, corner_drop, 0)
+    def corner_drop(block, target, base):
+        def drop(t, carry):
+            cols = tile_of(t)
+            target[base : base + cap, cols] = jnp.dot(
+                corner_act[block * cap : (block + 1) * cap, :],
+                corner_down[:, cols],
+                preferred_element_type=f32,
+            ).astype(bf16)
+            return carry
+
+        lax.fori_loop(0, model_dim // TILE, drop, 0)
+
+    corner_drop(1, corner_out, 0)
     mate_copy = remote(
-        corner_out, local_out.at[pl.ds(2 * cap, cap)], core_go.at[1], core_come.at[1], mate
+        corner_out, back.at[pl.ds(3 * cap, cap)], core_go.at[1], core_come.at[1], mate
     )
     mate_copy.start()
-    mate_copy.wait_recv()
-
-    def combine_local(t, carry):
-        cols = tile_of(t)
-        total[:, cols] = mixed[:, cols].astype(f32) + jnp.dot(
-            pick_local[...], local_out[:, cols], preferred_element_type=f32
-        )
-        return carry
-
-    lax.fori_loop(0, model_dim // TILE, combine_local, 0)
+    corner_drop(0, back, 2 * cap)
     for h, p in chunks:
         back_copy(h, p).wait_recv()
-
-    def combine_near(t, carry):
+    mate_copy.wait_recv()
+
+    def combine_rest(t, carry):
         cols = tile_of(t)
-        found = jnp.dot(pick_near[...], back[:, cols], preferred_element_type=f32)
+        found = jnp.dot(pick_rest[...], back[:, cols], preferred_element_type=f32)
         out_ref[:, cols] = (total[:, cols] + found).astype(bf16)
         return carry
 
-    lax.fori_loop(0, model_dim // TILE, combine_near, 0)
+    lax.fori_loop(0, model_dim // TILE, combine_rest, 0)
 
     for edge in edges:
         edge.wait_send()
@@ -792,19 +822,23 @@
     hidden = w_gate.shape[2]
     half = hidden // 2
     pool_w = w_up.shape[0]
-    cap = capacity(rows, routes.shape[1], count)
+    top = routes.shape[1]
+    cap = capacity(rows, top, count)
     vmem = pl.BlockSpec(memory_space=pltpu.VMEM)
-    anywhere = pl.BlockSpec(memory_space=pl.ANY)
     bf16, f32 = jnp.bfloat16, jnp.float32
+    hbm = functools.partial(pltpu.with_memory_space_constraint, memory_space=pltpu.HBM)
     dma = pltpu.SemaphoreType.DMA
     return pl.pallas_call(
         functools.partial(fused_kernel, count, tp_count),
         out_shape=jax.ShapeDtypeStruct((rows, model_dim), bf16),
-        in_specs=[anywhere] * 2 + [vmem] * 3 + [anywhere] * 7,
+        in_specs=[pl.BlockSpec(memory_space=pltpu.HBM)] * 12,
         out_specs=vmem,
         scratch_shapes=[
             pltpu.VMEM((channels, tok_dev + LANES), bf16),
             pltpu.VMEM((1, tok_dev + LANES), jnp.int32),
+            pltpu.VMEM((top, rows), jnp.int32),
+            pltpu.VMEM((top, rows), f32),
+            pltpu.VMEM((1, model_dim), f32),
             pltpu.VMEM((rows, model_dim), bf16),
             pltpu.VMEM((rows, model_dim), bf16),
             pltpu.VMEM(w_up.shape, bf16),
@@ -819,12 +853,12 @@
             pltpu.VMEM((rows, model_dim), bf16),
             pltpu.VMEM((rows, model_dim), bf16),
             pltpu.VMEM((2, 2 * cap, rows), bf16),
-            pltpu.VMEM((rows, 2 * cap), bf16),
-            pltpu.VMEM((rows, 3 * cap), bf16),
+            pltpu.VMEM((rows, cap), bf16),
+            pltpu.VMEM((rows, 4 * cap), bf16),
             pltpu.VMEM((2 * cap, model_dim), bf16),
             pltpu.VMEM((2 * cap, model_dim), bf16),
             pltpu.VMEM((2 * cap, model_dim), bf16),
-            pltpu.VMEM((2 * cap, model_dim), bf16),
+            pltpu.VMEM((4 * cap, model_dim), bf16),
             pltpu.VMEM((cap, model_dim), bf16),
             pltpu.VMEM((2 * cap, model_dim), bf16),
             pltpu.VMEM((cap, hidden), bf16),
@@ -832,16 +866,16 @@
             pltpu.VMEM((2, model_dim, half), bf16),
             pltpu.VMEM((half, model_dim), bf16),
             pltpu.VMEM((cap, model_dim), bf16),
-            pltpu.VMEM((3 * cap, model_dim), bf16),
+            pltpu.VMEM((cap, model_dim), bf16),
             pltpu.VMEM((rows, model_dim), f32),
-            dma((9,)),
+            dma((12,)),
             dma((2,)),
             dma((2,)),
             dma((tp_count,)),
             dma((tp_count,)),
-            dma((6,)),
-            dma((3, 6)),
-            dma((3, 6)),
+            dma((10,)),
+            dma((3, 10)),
+            dma((3, 10)),
             dma((4,)),
             dma((4,)),
             dma((4,)),
@@ -850,7 +884,7 @@
             dma((2,)),
         ],
         compiler_params=pltpu.CompilerParams(
-            collective_id=1, has_side_effects=True, vmem_limit_bytes=60 * 2**20
+            collective_id=1, has_side_effects=True, vmem_limit_bytes=52 * 2**20
         ),
         cost_estimate=pl.CostEstimate(
             flops=6 * count * cap * model_dim * hidden,
@@ -858,11 +892,11 @@
             transcendentals=count * cap * hidden,
         ),
     )(
-        pool_input.T,
-        docs[None, :],
-        routes.T,
-        route_weight.T,
-        g_ffn[None, :],
+        hbm(pool_input.T),
+        hbm(docs[None, :]),
+        hbm(routes.T),
+        hbm(route_weight.T),
+        hbm(g_ffn[None, :]),
         gate_pre,
         resid,
         w_up,

time: 75.4 us -> 67.7 us (0.90)
  Pallas kernels: 72.3 us -> 66 us
  local copies, waits for them, and re-layouts: 2.26 us -> 0.97 us
    pallas_call x1, Pallas kernels: 72.3 us -> 66 us  [run_fused(): pl.pallas_call(functools.partial(fused_kernel, count, tp_count), out_shap...]
    unnamed x1, local copies, waits for them, and re-layouts: 2.26 us -> 0.97 us
where the time goes in v1:
time: 67.7 us; the launch traced here: 67 us
  Pallas kernels  66 us (97%)
  local copies, waits for them, and re-layouts  0.97 us (1%)
    pallas_call x1, Pallas kernels, run_fused(): pl.pallas_call(functools.partial(fused_kernel, count, tp_count), out_shap...  66 us

profile of v1, /device:TPU:0, one launch (start us, length us, event | category | flops | bytes accessed | tf_op | source)
XLA Modules:
  0.0 67.0 jit_solution(690656718893595061)
XLA Ops:
  0.0 66.0 %shard_map.118 = bf16[512,1024]{1,0:T(8,128)(2,1)S(1)} custom-call(bf16[64,4096]{1,0:T(8,128)(2,1)} %bitcast.5, s32[1,4096]{1,0:T(1,128)} %bitcast.6, s32[2,512]{1,0:T(2,128)} %bitcast.7, f32[2,512]{1,0:T(2,128)} %bitcast.8, f32[1,1024]{1,0:T(1,128)} %bitcast.9, bf16[512,1024]{1,0:T(8,128)(2,1)} %gate_hbm.1, bf16[512,1024]{1,0:T(8,128)(2,1)} %resid_hbm.1, ...), custom_call_target="tpu_custom_call" | custom-call | flops 8053063680 | bytes 6291456 | tf_op jit(solution)/shard_map/pallas_call | solution.py:831
  66.0 1.0 %copy.14 = bf16[512,1024]{1,0:T(8,128)(2,1)} copy(bf16[512,1024]{1,0:T(8,128)(2,1)S(1)} %shard_map.118) | data formatting | bytes 2097152

commit v2 on v1

--- a/solution.py
+++ b/solution.py
@@ -11,7 +11,8 @@
 RIM = 15
 TILE = 256
 LANES = 128
-END_SHARE = 6
+UNIT = 16
+END_SHARE = (11, 11, 12)
 MESH = pl.DeviceIdType.MESH
 
 
@@ -325,6 +326,10 @@
     out_come,
     ret_go,
     ret_come,
+    late_go,
+    late_come,
+    mate_go,
+    mate_come,
     core_go,
     core_come,
 ):
@@ -347,6 +352,9 @@
             (
                 (pool_hbm, pool.at[:, LANES:]),
                 (docs_hbm, docs.at[:, LANES:]),
+                (w_gate_hbm.at[0], w_gate),
+                (w_lift_hbm.at[0], w_lift),
+                (w_down_hbm.at[0], w_down),
                 (routes_hbm, routes_ref),
                 (route_weight_hbm, route_weight_ref),
                 (w_up_hbm, w_up),
@@ -354,13 +362,10 @@
                 (w_out_hbm, w_out),
                 (resid_hbm, resid),
                 (gain_hbm, gain),
-                (w_gate_hbm.at[0], w_gate),
-                (w_lift_hbm.at[0], w_lift),
-                (w_down_hbm.at[0], w_down),
             )
         )
     ]
-    for load in loads[:2]:
+    for load in loads:
         load.start()
     barrier = pltpu.get_barrier_semaphore()
 
@@ -378,9 +383,6 @@
 
     lax.fori_loop(1, count, greet_sp, 0)
     lax.fori_loop(1, tp_count, greet_tp, 0)
-    for load in loads[2:]:
-        load.start()
-
     def remote(src, dst, go, come, device):
         return pltpu.make_async_remote_copy(
             src_ref=src,
@@ -404,72 +406,93 @@
         for i, ref in enumerate((pool, docs))
     ]
 
-    parts = [(m, q) for q in range(4) for m in range(2)] + [(2, q) for q in range(2)]
-    sources = (w_gate_hbm, w_lift_hbm, w_down_hbm)
-    inner = (16 - END_SHARE) // 2
+    pieces = [(m, q) for q in range(4) for m in range(2)] + [(2, q) for q in range(4)]
+    sources = (w_gate, w_lift, w_down)
+    far = partner(sp, 3, count)
 
     def span(m, q, zone):
-        unit, cuts = (model_dim // 16, 4) if m < 2 else (half // 16, 2)
-        if isinstance(zone, int) and zone == 0:
-            return q * (END_SHARE * unit // cuts), END_SHARE * unit // cuts
-        start = (END_SHARE + inner * (zone - 1)) * unit + q * (inner * unit // cuts)
-        return pl.multiple_of(start, 16), inner * unit // cuts
-
-    def place(m, start, size):
+        units = (model_dim if m < 2 else half) // UNIT
+        ends = units * END_SHARE[m] // 32
+        inner = (units - ends) // 2
+        is_end = isinstance(zone, int) and zone == 0
+        size = ends if is_end else inner
+        low, high = (q * size // 4, (q + 1) * size // 4) if m < 2 else (0, size)
+        if is_end:
+            return low * UNIT, (high - low) * UNIT
+        start = (ends + inner * (zone - 1) + low) * UNIT
+        return pl.multiple_of(start, UNIT), (high - low) * UNIT
+
+    def place(m, q, start, size):
         if m < 2:
             return corner_up.at[m, pl.ds(start, size), :]
-        return corner_down.at[pl.ds(start, size), :]
+        return corner_down.at[pl.ds(start, size), pl.ds(q * TILE, TILE)]
 
     def fetch(i, zone):
-        m, q = parts[i]
+        m, q = pieces[i]
         start, size = span(m, q, zone)
         if m < 2:
             cols = pl.ds(pl.multiple_of(core * half, half), half)
-            src = sources[m].at[0, pl.ds(start, size), cols]
+            src = sources[m].at[pl.ds(start, size), cols]
         else:
-            first = pl.multiple_of(core * half + start, 16)
-            src = sources[m].at[0, pl.ds(first, size), :]
+            first = pl.multiple_of(core * half + start, UNIT)
+            src = sources[m].at[pl.ds(first, size), pl.ds(q * TILE, TILE)]
         return remote(
             src,
-            place(m, start, size),
+            place(m, q, start, size),
             part_go.at[i],
             part_come.at[zone, i],
-            {"sp": partner(sp, 3, count)},
-        )
-
-    def share(i, zone, hop):
-        m, q = parts[i]
+            {"sp": far},
+        )
+
+    def share(i, zone, way):
+        m, q = pieces[i]
         start, size = span(m, q, zone)
         return remote(
-            place(m, start, size),
-            place(m, start, size),
-            share_go.at[hop - 1, i],
+            place(m, q, start, size),
+            place(m, q, start, size),
+            share_go.at[way, i],
             part_come.at[zone, i],
-            {"tp": partner(tp, 2 * hop, tp_count)},
+            {"tp": partner(tp, 6 if way == 1 else 2, tp_count)},
         )
 
     def pass_on(i):
         @pl.when(at_end)
         def _():
             fetch(i, 0).wait_recv()
-            share(i, 0, 1).start()
+            share(i, 0, 0).start()
 
         @pl.when(inside)
         def _():
             fetch(i, plane).wait_recv()
-            for hop in (3, 2, 1):
-                share(i, plane, hop).start()
+            share(i, plane, 1).start()
+            share(i, plane, 0).start()
+
+    def relay(i):
+        @pl.when(inside)
+        def _():
+            share(i, 3 - plane, 1).wait_recv()
+            share(i, 3 - plane, 2).start()
 
     def arrived(i):
         @pl.when(at_end)
         def _():
-            share(i, 1, 1).wait_recv()
-            share(i, 2, 1).wait_recv()
+            share(i, 1, 0).wait_recv()
+            share(i, 2, 0).wait_recv()
 
         @pl.when(inside)
         def _():
-            share(i, 0, 1).wait_recv()
-            share(i, 3 - plane, 1).wait_recv()
+            share(i, 0, 0).wait_recv()
+
+    def fetch_all(some):
+        @pl.when(at_end)
+        def _():
+            for i in some:
+                fetch(i, 0).start()
+
+        @pl.when(inside)
+        def _():
+            for i in some:
+                fetch(i, plane).start()
 
     for load in loads[:2]:
         load.wait()
@@ -477,15 +500,9 @@
     for edge in edges:
         edge.start()
 
-    @pl.when(at_end)
-    def _():
-        for i in range(len(parts)):
-            fetch(i, 0).start()
-
-    @pl.when(inside)
-    def _():
-        for i in range(len(parts)):
-            fetch(i, plane).start()
+    for load in loads[2:4]:
+        load.wait()
+    fetch_all(range(8))
 
     level = (tp * channels) // (channels * tp_count // 4)
 
@@ -531,6 +548,8 @@
         return carry
 
     lax.fori_loop(0, tp_count - 1, pool_step, 0)
+    loads[4].wait()
+    fetch_all(range(8, 12))
     for edge in edges:
         edge.wait_recv()
 
@@ -541,7 +560,7 @@
     gathered[pl.ds(pl.multiple_of(tp * channels, channels), channels), :] = pool_block(0)
     pass_on(0)
 
-    for load in loads[2:4]:
+    for load in loads[5:7]:
         load.wait()
 
     first, second = routes_ref[0:1, :], routes_ref[1:2, :]
@@ -592,7 +611,7 @@
     for i in range(1, 4):
         pass_on(i)
 
-    for load in loads[4:9]:
+    for load in loads[7:]:
         load.wait()
 
     def pool_wait(j, carry):
@@ -648,13 +667,23 @@
             {"sp": partner(sp, p + 1, count)},
         )
 
-    def back_copy(h, p):
-        block = pl.ds((2 * h + p) * part, part)
+    def back_copy(p):
+        block = pl.ds(p * part, part)
         return remote(
             result.at[block],
             back.at[block],
-            ret_go.at[2 * h + p],
-            ret_come.at[2 * h + p],
+            ret_go.at[p],
+            ret_come.at[p],
+            {"sp": partner(sp, p + 1, count)},
+        )
+
+    def late_copy(p, t):
+        block = pl.ds((2 + p) * part, part)
+        return remote(
+            result.at[block, tile_of(t)],
+            back.at[block, tile_of(t)],
+            late_go.at[p, t],
+            late_come.at[p, t],
             {"sp": partner(sp, p + 1, count)},
         )
 
@@ -684,7 +713,7 @@
         lift = jnp.clip(lift, -7.0, 7.0)
         return ((lift + 1.0) * gate * jax.nn.sigmoid(1.702 * gate)).astype(bf16)
 
-    def ffn(source, target, base):
+    def ffn(source, target, base, then=lambda t: None):
         def up(t, carry):
             cols = tile_of(t)
             x = source[base : base + cap, :]
@@ -701,14 +730,14 @@
             target[base : base + cap, cols] = jnp.dot(
                 act[...], w_down[:, cols], preferred_element_type=f32
             ).astype(bf16)
+            then(t)
             return carry
 
         lax.fori_loop(0, model_dim // TILE, down, 0)
 
-    for load in loads[9:]:
-        load.wait()
     ffn(own, local_out, 0)
     pass_on(8)
+    pass_on(9)
 
     def combine_own(t, carry):
         cols = tile_of(t)
@@ -718,14 +747,26 @@
         return carry
 
     lax.fori_loop(0, model_dim // TILE, combine_own, 0)
-    pass_on(9)
-
-    for h in range(2):
+    pass_on(10)
+    pass_on(11)
+    for i in range(8):
+        relay(i)
+
+    for p in range(2):
+        out_copy(0, p).wait_recv()
+    ffn(recv, result, 0)
+    for p in range(2):
+        back_copy(p).start()
+    for i in range(8, 12):
+        relay(i)
+    for p in range(2):
+        out_copy(1, p).wait_recv()
+
+    def send_back(t):
         for p in range(2):
-            out_copy(h, p).wait_recv()
-        ffn(recv, result, h * cap)
-        for p in range(2):
-            back_copy(h, p).start()
+            late_copy(p, t).start()
+
+    ffn(recv, result, cap, send_back)
 
     corner_copy.wait_recv()
     for i in range(8):
@@ -741,38 +782,43 @@
         return carry
 
     lax.fori_loop(0, half // TILE, corner_lift, 0)
-    for i in range(8, 10):
-        arrived(i)
-
-    def corner_drop(block, target, base):
-        def drop(t, carry):
-            cols = tile_of(t)
+    def mate_copy(t):
+        return remote(
+            corner_out.at[:, tile_of(t)],
+            back.at[pl.ds(3 * cap, cap), tile_of(t)],
+            mate_go.at[t],
+            mate_come.at[t],
+            mate,
+        )
+
+    def corner_drop(t):
+        cols = tile_of(t)
+        for block, target, base in ((1, corner_out, 0), (0, back, 2 * cap)):
             target[base : base + cap, cols] = jnp.dot(
                 corner_act[block * cap : (block + 1) * cap, :],
                 corner_down[:, cols],
                 preferred_element_type=f32,
             ).astype(bf16)
-            return carry
-
-        lax.fori_loop(0, model_dim // TILE, drop, 0)
-
-    corner_drop(1, corner_out, 0)
-    mate_copy = remote(
-        corner_out, back.at[pl.ds(3 * cap, cap)], core_go.at[1], core_come.at[1], mate
-    )
-    mate_copy.start()
-    corner_drop(0, back, 2 * cap)
-    for h, p in chunks:
-        back_copy(h, p).wait_recv()
-    mate_copy.wait_recv()
-
-    def combine_rest(t, carry):
+            if block == 1:
+                mate_copy(t).start()
+
+    def combine_rest(t):
         cols = tile_of(t)
+        for p in range(2):
+            late_copy(p, t).wait_recv()
+        mate_copy(t).wait_recv()
         found = jnp.dot(pick_rest[...], back[:, cols], preferred_element_type=f32)
         out_ref[:, cols] = (total[:, cols] + found).astype(bf16)
-        return carry
-
-    lax.fori_loop(0, model_dim // TILE, combine_rest, 0)
+
+    tiles = model_dim // TILE
+    for p in range(2):
+        back_copy(p).wait_recv()
+    for t in range(tiles):
+        arrived(8 + t)
+        corner_drop(t)
+        if t > 0:
+            combine_rest(t - 1)
+    combine_rest(tiles - 1)
 
     for edge in edges:
         edge.wait_send()
@@ -784,21 +830,31 @@
     lax.fori_loop(1, tp_count, pool_sent, 0)
     for h, p in chunks:
         out_copy(h, p).wait_send()
-        back_copy(h, p).wait_send()
     corner_copy.wait_send()
-    mate_copy.wait_send()
-    for i in range(len(parts)):
-
-        @pl.when(at_end)
-        def _():
+    for p in range(2):
+        back_copy(p).wait_send()
+
+    def late_sent(t, carry):
+        mate_copy(t).wait_send()
+        for p in range(2):
+            late_copy(p, t).wait_send()
+        return carry
+
+    lax.fori_loop(0, tiles, late_sent, 0)
+
+    @pl.when(at_end)
+    def _():
+        for i in range(len(pieces)):
             fetch(i, 0).wait_send()
-            share(i, 0, 1).wait_send()
-
-        @pl.when(inside)
-        def _():
+            share(i, 0, 0).wait_send()
+
+    @pl.when(inside)
+    def _():
+        for i in range(len(pieces)):
             fetch(i, plane).wait_send()
-            for hop in (1, 2, 3):
-                share(i, plane, hop).wait_send()
+            for way in range(2):
+                share(i, plane, way).wait_send()
+            share(i, 3 - plane, 2).wait_send()
 
 
 def run_fused(
@@ -873,15 +929,19 @@
             dma((2,)),
             dma((tp_count,)),
             dma((tp_count,)),
-            dma((10,)),
-            dma((3, 10)),
-            dma((3, 10)),
-            dma((4,)),
-            dma((4,)),
+            dma((12,)),
+            dma((3, 12)),
+            dma((3, 12)),
             dma((4,)),
             dma((4,)),
             dma((2,)),
             dma((2,)),
+            dma((2, 4)),
+            dma((2, 4)),
+            dma((4,)),
+            dma((4,)),
+            dma((1,)),
+            dma((1,)),
         ],
         compiler_params=pltpu.CompilerParams(
             collective_id=1, has_side_effects=True, vmem_limit_bytes=52 * 2**20

time: 67.7 us -> 65.7 us (0.970)
  Pallas kernels: 66 us -> 64.6 us
    pallas_call x1, Pallas kernels: 66 us -> 64.6 us  [run_fused(): pl.pallas_call(functools.partial(fused_kernel, count, tp_count), out_shap...]
where the time goes in v2:
time: 65.7 us; the launch traced here: 65.5 us
  Pallas kernels  64.6 us (98%)
  local copies, waits for them, and re-layouts  0.97 us (1%)
    pallas_call x1, Pallas kernels, run_fused(): pl.pallas_call(functools.partial(fused_kernel, count, tp_count), out_shap...  64.6 us

profile of v2, /device:TPU:0, one launch (start us, length us, event | category | flops | bytes accessed | tf_op | source)
XLA Modules:
  0.0 65.5 jit_solution(16728197920557539666)
XLA Ops:
  0.0 64.6 %shard_map.118 = bf16[512,1024]{1,0:T(8,128)(2,1)S(1)} custom-call(bf16[64,4096]{1,0:T(8,128)(2,1)} %bitcast.5, s32[1,4096]{1,0:T(1,128)} %bitcast.6, s32[2,512]{1,0:T(2,128)} %bitcast.7, f32[2,512]{1,0:T(2,128)} %bitcast.8, f32[1,1024]{1,0:T(1,128)} %bitcast.9, bf16[512,1024]{1,0:T(8,128)(2,1)} %gate_hbm.1, bf16[512,1024]{1,0:T(8,128)(2,1)} %resid_hbm.1, ...), custom_call_target="tpu_custom_call" | custom-call | flops 8053063680 | bytes 6291456 | tf_op jit(solution)/shard_map/pallas_call | solution.py:887
  64.6 1.0 %copy.14 = bf16[512,1024]{1,0:T(8,128)(2,1)} copy(bf16[512,1024]{1,0:T(8,128)(2,1)S(1)} %shard_map.118) | data formatting | bytes 2097152

commit v3 on v2

--- a/solution.py
+++ b/solution.py
@@ -300,6 +300,7 @@
     normed,
     onehot,
     pick_own,
+    pick_near,
     pick_rest,
     send,
     recv,
@@ -320,8 +321,10 @@
     pool_go,
     pool_come,
     part_go,
-    part_come,
+    direct_come,
     share_go,
+    near_come,
+    middle_come,
     out_go,
     out_come,
     ret_go,
@@ -393,6 +396,7 @@
             device_id_type=MESH,
         )
 
+    mate = {"tp": partner(tp, 1, tp_count)}
     following = {"sp": lax.rem(sp + 1, count)}
     tok_dev = pool_hbm.shape[1]
     edges = [
@@ -439,8 +443,8 @@
         return remote(
             src,
             place(m, q, start, size),
-            part_go.at[i],
-            part_come.at[zone, i],
+            part_go.at[m // 2],
+            direct_come.at[i],
             {"sp": far},
         )
 
@@ -450,8 +454,8 @@
         return remote(
             place(m, q, start, size),
             place(m, q, start, size),
-            share_go.at[way, i],
-            part_come.at[zone, i],
+            share_go.at[way, m // 2],
+            middle_come.at[i] if way == 1 else near_come.at[way // 2, max(i - 7, 0)],
             {"tp": partner(tp, 6 if way == 1 else 2, tp_count)},
         )
 
@@ -473,11 +477,30 @@
             share(i, 3 - plane, 1).wait_recv()
             share(i, 3 - plane, 2).start()
 
+    def whole(zone, down):
+        start, size = span(2 if down else 0, 0, zone)
+        if down:
+            return corner_down.at[pl.ds(start, size), :]
+        size = sum(span(0, q, zone)[1] for q in range(4))
+        return corner_up.at[:, pl.ds(start, size), :]
+
+    def up_arrived():
+        @pl.when(at_end)
+        def _():
+            for way, zone in ((0, 1), (2, 2)):
+                ref = whole(zone, False)
+                remote(ref, ref, share_go.at[0, 0], near_come.at[way // 2, 0], mate).wait_recv()
+
+        @pl.when(inside)
+        def _():
+            ref = whole(0, False)
+            remote(ref, ref, share_go.at[0, 0], near_come.at[0, 0], mate).wait_recv()
+
     def arrived(i):
         @pl.when(at_end)
         def _():
             share(i, 1, 0).wait_recv()
-            share(i, 2, 0).wait_recv()
+            share(i, 2, 2).wait_recv()
 
         @pl.when(inside)
         def _():
@@ -510,8 +533,8 @@
         return remote(
             pooled.at[j],
             gathered.at[pl.ds(pl.multiple_of(tp * channels, channels), channels), :],
-            pool_go.at[j],
-            pool_come.at[j],
+            pool_go.at[0],
+            pool_come.at[0],
             {"tp": partner(tp, j, tp_count)},
         )
 
@@ -603,9 +626,11 @@
 
     slots = lax.broadcasted_iota(jnp.int32, (rows, cap), 1)
     pick_own[...] = weighed(slots, 0, 0).astype(bf16)
-    slots = lax.broadcasted_iota(jnp.int32, (rows, 4 * cap), 1)
-    found = weighed(slots, 1, 0) + weighed(slots, 2, 0)
-    found = found + weighed(slots, 3, cap) + weighed(slots, 3, 2 * cap)
+    pick_near[...] = (weighed(slots, 1, 0) + weighed(slots, 2, 0)).astype(bf16)
+    slots = lax.broadcasted_iota(jnp.int32, (rows, 3 * cap), 1)
+    found = weighed(slots, 3, -cap) + weighed(slots, 3, 0)
+    late = jnp.where(slots >= 2 * cap, slots - cap, -1)
+    found = found + weighed(late, 1, 0) + weighed(late, 2, 0)
     pick_rest[...] = found.astype(bf16)
 
     for i in range(1, 4):
@@ -614,11 +639,8 @@
     for load in loads[7:]:
         load.wait()
 
-    def pool_wait(j, carry):
-        pool_copy(j).wait_recv()
-        return carry
-
-    lax.fori_loop(1, tp_count, pool_wait, 0)
+    others = gathered.at[pl.ds(0, (tp_count - 1) * channels), :]
+    remote(others, others, pool_go.at[0], pool_come.at[0], mate).wait_recv()
     tokens[...] = gathered[...].T
 
     def lift_up(t, carry):
@@ -662,8 +684,8 @@
         return remote(
             send.at[block],
             recv.at[block],
-            out_go.at[2 * h + p],
-            out_come.at[2 * h + p],
+            out_go.at[0],
+            out_come.at[h],
             {"sp": partner(sp, p + 1, count)},
         )
 
@@ -672,18 +694,17 @@
         return remote(
             result.at[block],
             back.at[block],
-            ret_go.at[p],
-            ret_come.at[p],
+            ret_go.at[0],
+            ret_come.at[0],
             {"sp": partner(sp, p + 1, count)},
         )
 
     def late_copy(p, t):
-        block = pl.ds((2 + p) * part, part)
         return remote(
-            result.at[block, tile_of(t)],
-            back.at[block, tile_of(t)],
-            late_go.at[p, t],
-            late_come.at[p, t],
+            result.at[pl.ds((2 + p) * part, part), tile_of(t)],
+            back.at[pl.ds(3 * cap + p * part, part), tile_of(t)],
+            late_go.at[0],
+            late_come.at[t],
             {"sp": partner(sp, p + 1, count)},
         )
 
@@ -701,7 +722,6 @@
         return carry
 
     lax.fori_loop(0, model_dim // TILE, pack_local, 0)
-    mate = {"tp": partner(tp, 1, tp_count)}
     corner_copy = remote(
         corner.at[pl.ds(0, cap)], corner.at[pl.ds(cap, cap)], core_go.at[0], core_come.at[0], mate
     )
@@ -752,15 +772,17 @@
     for i in range(8):
         relay(i)
 
-    for p in range(2):
-        out_copy(0, p).wait_recv()
+    def near_arrived(h):
+        block = pl.ds(h * cap, cap)
+        remote(send.at[block], recv.at[block], out_go.at[0], out_come.at[h], mate).wait_recv()
+
+    near_arrived(0)
     ffn(recv, result, 0)
     for p in range(2):
         back_copy(p).start()
     for i in range(8, 12):
         relay(i)
-    for p in range(2):
-        out_copy(1, p).wait_recv()
+    near_arrived(1)
 
     def send_back(t):
         for p in range(2):
@@ -769,8 +791,7 @@
     ffn(recv, result, cap, send_back)
 
     corner_copy.wait_recv()
-    for i in range(8):
-        arrived(i)
+    up_arrived()
 
     def corner_lift(t, carry):
         cols = tile_of(t)
@@ -785,15 +806,15 @@
     def mate_copy(t):
         return remote(
             corner_out.at[:, tile_of(t)],
-            back.at[pl.ds(3 * cap, cap), tile_of(t)],
-            mate_go.at[t],
+            back.at[pl.ds(2 * cap, cap), tile_of(t)],
+            mate_go.at[0],
             mate_come.at[t],
             mate,
         )
 
     def corner_drop(t):
         cols = tile_of(t)
-        for block, target, base in ((1, corner_out, 0), (0, back, 2 * cap)):
+        for block, target, base in ((1, corner_out, 0), (0, back, cap)):
             target[base : base + cap, cols] = jnp.dot(
                 corner_act[block * cap : (block + 1) * cap, :],
                 corner_down[:, cols],
@@ -802,17 +823,24 @@
             if block == 1:
                 mate_copy(t).start()
 
+    def combine_near(t, carry):
+        cols = tile_of(t)
+        found = jnp.dot(pick_near[...], back[0:cap, cols], preferred_element_type=f32)
+        total[:, cols] = total[:, cols] + found
+        return carry
+
     def combine_rest(t):
         cols = tile_of(t)
-        for p in range(2):
-            late_copy(p, t).wait_recv()
         mate_copy(t).wait_recv()
-        found = jnp.dot(pick_rest[...], back[:, cols], preferred_element_type=f32)
+        block = back.at[pl.ds(3 * cap, cap), cols]
+        remote(block, block, late_go.at[0], late_come.at[t], mate).wait_recv()
+        found = jnp.dot(pick_rest[...], back[cap:, cols], preferred_element_type=f32)
         out_ref[:, cols] = (total[:, cols] + found).astype(bf16)
 
     tiles = model_dim // TILE
-    for p in range(2):
-        back_copy(p).wait_recv()
+    block = pl.ds(0, cap)
+    remote(result.at[block], back.at[block], ret_go.at[0], ret_come.at[0], mate).wait_recv()
+    lax.fori_loop(0, tiles, combine_near, 0)
     for t in range(tiles):
         arrived(8 + t)
         corner_drop(t)
@@ -823,38 +851,32 @@
     for edge in edges:
         edge.wait_send()
 
-    def pool_sent(j, carry):
-        pool_copy(j).wait_send()
-        return carry
-
-    lax.fori_loop(1, tp_count, pool_sent, 0)
-    for h, p in chunks:
-        out_copy(h, p).wait_send()
+    others = pooled.at[pl.ds(1, tp_count - 1)]
+    remote(others, others, pool_go.at[0], pool_come.at[0], mate).wait_send()
+    remote(send, recv, out_go.at[0], out_come.at[0], mate).wait_send()
     corner_copy.wait_send()
-    for p in range(2):
-        back_copy(p).wait_send()
-
-    def late_sent(t, carry):
-        mate_copy(t).wait_send()
-        for p in range(2):
-            late_copy(p, t).wait_send()
-        return carry
-
-    lax.fori_loop(0, tiles, late_sent, 0)
+    block = pl.ds(0, cap)
+    remote(result.at[block], back.at[block], ret_go.at[0], ret_come.at[0], mate).wait_send()
+    block = pl.ds(cap, cap)
+    remote(result.at[block], back.at[block], late_go.at[0], late_come.at[0], mate).wait_send()
+    remote(corner_out, corner_out, mate_go.at[0], mate_come.at[0], mate).wait_send()
+
+    def gone(ref, sem):
+        remote(ref, ref, sem, direct_come.at[0], mate).wait_send()
 
     @pl.when(at_end)
     def _():
-        for i in range(len(pieces)):
-            fetch(i, 0).wait_send()
-            share(i, 0, 0).wait_send()
+        for k in range(2):
+            gone(whole(0, k), part_go.at[k])
+            gone(whole(0, k), share_go.at[0, k])
 
     @pl.when(inside)
     def _():
-        for i in range(len(pieces)):
-            fetch(i, plane).wait_send()
-            for way in range(2):
-                share(i, plane, way).wait_send()
-            share(i, 3 - plane, 2).wait_send()
+        for k in range(2):
+            gone(whole(plane, k), part_go.at[k])
+            gone(whole(plane, k), share_go.at[0, k])
+            gone(whole(plane, k), share_go.at[1, k])
+            gone(whole(3 - plane, k), share_go.at[2, k])
 
 
 def run_fused(
@@ -910,7 +932,8 @@
             pltpu.VMEM((rows, model_dim), bf16),
             pltpu.VMEM((2, 2 * cap, rows), bf16),
             pltpu.VMEM((rows, cap), bf16),
-            pltpu.VMEM((rows, 4 * cap), bf16),
+            pltpu.VMEM((rows, cap), bf16),
+            pltpu.VMEM((rows, 3 * cap), bf16),
             pltpu.VMEM((2 * cap, model_dim), bf16),
             pltpu.VMEM((2 * cap, model_dim), bf16),
             pltpu.VMEM((2 * cap, model_dim), bf16),
@@ -927,18 +950,20 @@
             dma((12,)),
             dma((2,)),
             dma((2,)),
-            dma((tp_count,)),
-            dma((tp_count,)),
+            dma((1,)),
+            dma((1,)),
+            dma((2,)),
             dma((12,)),
-            dma((3, 12)),
-            dma((3, 12)),
+            dma((3, 2)),
+            dma((2, 5)),
+            dma((12,)),
+            dma((1,)),
+            dma((2,)),
+            dma((1,)),
+            dma((1,)),
+            dma((1,)),
             dma((4,)),
-            dma((4,)),
-            dma((2,)),
-            dma((2,)),
-            dma((2, 4)),
-            dma((2, 4)),
-            dma((4,)),
+            dma((1,)),
             dma((4,)),
             dma((1,)),
             dma((1,)),

time: 65.7 us -> 64.7 us (0.985)
  Pallas kernels: 64.6 us -> 63.6 us
    pallas_call x1, Pallas kernels: 64.6 us -> 63.6 us  [run_fused(): pl.pallas_call(functools.partial(fused_kernel, count, tp_count), out_shap...]
where the time goes in v3:
time: 64.7 us; the launch traced here: 64.6 us
  Pallas kernels  63.6 us (98%)
  local copies, waits for them, and re-layouts  0.97 us (1%)
    pallas_call x1, Pallas kernels, run_fused(): pl.pallas_call(functools.partial(fused_kernel, count, tp_count), out_shap...  63.6 us

profile of v3, /device:TPU:0, one launch (start us, length us, event | category | flops | bytes accessed | tf_op | source)
XLA Modules:
  0.0 64.6 jit_solution(8866060742912148307)
XLA Ops:
  0.0 63.6 %shard_map.118 = bf16[512,1024]{1,0:T(8,128)(2,1)S(1)} custom-call(bf16[64,4096]{1,0:T(8,128)(2,1)} %bitcast.5, s32[1,4096]{1,0:T(1,128)} %bitcast.6, s32[2,512]{1,0:T(2,128)} %bitcast.7, f32[2,512]{1,0:T(2,128)} %bitcast.8, f32[1,1024]{1,0:T(1,128)} %bitcast.9, bf16[512,1024]{1,0:T(8,128)(2,1)} %gate_hbm.1, bf16[512,1024]{1,0:T(8,128)(2,1)} %resid_hbm.1, ...), custom_call_target="tpu_custom_call" | custom-call | flops 8053063680 | bytes 6291456 | tf_op jit(solution)/shard_map/pallas_call | solution.py:909
  63.6 1.0 %copy.14 = bf16[512,1024]{1,0:T(8,128)(2,1)} copy(bf16[512,1024]{1,0:T(8,128)(2,1)S(1)} %shard_map.118) | data formatting | bytes 2097152

commit v4 on v3

--- a/solution.py
+++ b/solution.py
@@ -262,6 +262,15 @@
         w_lift,
         w_down,
     )
+
+
+def halves_dot(rows, weights):
+    half = rows.shape[0] // 2
+    parts = [
+        jnp.dot(part, weights, preferred_element_type=jnp.float32)
+        for part in (rows[:half], rows[half:])
+    ]
+    return jnp.concatenate(parts, axis=0)
 
 
 def fused_kernel(
@@ -368,7 +377,7 @@
             )
         )
     ]
-    for load in loads:
+    for load in loads[:5]:
         load.start()
     barrier = pltpu.get_barrier_semaphore()
 
@@ -420,7 +429,7 @@
         inner = (units - ends) // 2
         is_end = isinstance(zone, int) and zone == 0
         size = ends if is_end else inner
-        low, high = (q * size // 4, (q + 1) * size // 4) if m < 2 else (0, size)
+        low, high = (q % 2 * size // 2, (q % 2 + 1) * size // 2) if m < 2 else (0, size)
         if is_end:
             return low * UNIT, (high - low) * UNIT
         start = (ends + inner * (zone - 1) + low) * UNIT
@@ -428,14 +437,14 @@
 
     def place(m, q, start, size):
         if m < 2:
-            return corner_up.at[m, pl.ds(start, size), :]
+            return corner_up.at[m, pl.ds(start, size), tile_of(q // 2)]
         return corner_down.at[pl.ds(start, size), pl.ds(q * TILE, TILE)]
 
     def fetch(i, zone):
         m, q = pieces[i]
         start, size = span(m, q, zone)
         if m < 2:
-            cols = pl.ds(pl.multiple_of(core * half, half), half)
+            cols = pl.ds(pl.multiple_of(core * half + q // 2 * TILE, TILE), TILE)
             src = sources[m].at[pl.ds(start, size), cols]
         else:
             first = pl.multiple_of(core * half + start, UNIT)
@@ -455,7 +464,7 @@
             place(m, q, start, size),
             place(m, q, start, size),
             share_go.at[way, m // 2],
-            middle_come.at[i] if way == 1 else near_come.at[way // 2, max(i - 7, 0)],
+            middle_come.at[i] if way == 1 else near_come.at[way // 2, i // 4 if i < 8 else i - 6],
             {"tp": partner(tp, 6 if way == 1 else 2, tp_count)},
         )
 
@@ -481,20 +490,22 @@
         start, size = span(2 if down else 0, 0, zone)
         if down:
             return corner_down.at[pl.ds(start, size), :]
-        size = sum(span(0, q, zone)[1] for q in range(4))
+        size = sum(span(0, q, zone)[1] for q in range(2))
         return corner_up.at[:, pl.ds(start, size), :]
 
-    def up_arrived():
+    def up_arrived(u):
+        def wait_for(zone, kind):
+            ref = whole(zone, False).at[:, :, tile_of(u)]
+            remote(ref, ref, share_go.at[0, 0], near_come.at[kind, u], mate).wait_recv()
+
         @pl.when(at_end)
         def _():
-            for way, zone in ((0, 1), (2, 2)):
-                ref = whole(zone, False)
-                remote(ref, ref, share_go.at[0, 0], near_come.at[way // 2, 0], mate).wait_recv()
+            wait_for(1, 0)
+            wait_for(2, 1)
 
         @pl.when(inside)
         def _():
-            ref = whole(0, False)
-            remote(ref, ref, share_go.at[0, 0], near_come.at[0, 0], mate).wait_recv()
+            wait_for(0, 0)
 
     def arrived(i):
         @pl.when(at_end)
@@ -526,6 +537,8 @@
     for load in loads[2:4]:
         load.wait()
     fetch_all(range(8))
+    for load in loads[5:]:
+        load.start()
 
     level = (tp * channels) // (channels * tp_count // 4)
 
@@ -645,7 +658,7 @@
 
     def lift_up(t, carry):
         cols = tile_of(t)
-        lifted = jnp.dot(tokens[...], w_up[:, cols], preferred_element_type=f32)
+        lifted = halves_dot(tokens[...], w_up[:, cols])
         gated[:, cols] = (jax.nn.sigmoid(gate_pre[:, cols].astype(f32)) * lifted).astype(bf16)
         return carry
 
@@ -653,7 +666,7 @@
 
     def mix(t, carry):
         cols = tile_of(t)
-        added = jnp.dot(gated[...], w_out[:, cols], preferred_element_type=f32)
+        added = halves_dot(gated[...], w_out[:, cols])
         mixed[:, cols] = (resid[:, cols].astype(f32) + added).astype(bf16)
         return carry
 
@@ -672,9 +685,7 @@
 
     def pack_near(t, carry):
         cols = tile_of(t)
-        send[:, cols] = jnp.dot(
-            onehot[0], normed[:, cols], preferred_element_type=f32
-        ).astype(bf16)
+        send[:, cols] = halves_dot(onehot[0], normed[:, cols]).astype(bf16)
         return carry
 
     lax.fori_loop(0, model_dim // TILE, pack_near, 0)
@@ -716,7 +727,7 @@
 
     def pack_local(t, carry):
         cols = tile_of(t)
-        packed = jnp.dot(onehot[1], normed[:, cols], preferred_element_type=f32).astype(bf16)
+        packed = halves_dot(onehot[1], normed[:, cols]).astype(bf16)
         own[:, cols] = packed[:cap]
         corner[0:cap, cols] = packed[cap:]
         return carry
@@ -747,9 +758,7 @@
 
         def down(t, carry):
             cols = tile_of(t)
-            target[base : base + cap, cols] = jnp.dot(
-                act[...], w_down[:, cols], preferred_element_type=f32
-            ).astype(bf16)
+            target[base : base + cap, cols] = halves_dot(act[...], w_down[:, cols]).astype(bf16)
             then(t)
             return carry
 
@@ -761,9 +770,8 @@
 
     def combine_own(t, carry):
         cols = tile_of(t)
-        total[:, cols] = mixed[:, cols].astype(f32) + jnp.dot(
-            pick_own[...], local_out[:, cols], preferred_element_type=f32
-        )
+        found = halves_dot(pick_own[...], local_out[:, cols])
+        total[:, cols] = mixed[:, cols].astype(f32) + found
         return carry
 
     lax.fori_loop(0, model_dim // TILE, combine_own, 0)
@@ -791,18 +799,31 @@
     ffn(recv, result, cap, send_back)
 
     corner_copy.wait_recv()
-    up_arrived()
-
-    def corner_lift(t, carry):
+
+    def corner_lift(t):
         cols = tile_of(t)
         x = corner[...]
         corner_act[:, cols] = activate(
             jnp.dot(x, corner_up[0, :, cols], preferred_element_type=f32),
             jnp.dot(x, corner_up[1, :, cols], preferred_element_type=f32),
         )
-        return carry
-
-    lax.fori_loop(0, half // TILE, corner_lift, 0)
+
+    def combine_near(t, carry):
+        cols = tile_of(t)
+        found = halves_dot(pick_near[...], back[0:cap, cols])
+        total[:, cols] = total[:, cols] + found
+        return carry
+
+    tiles = model_dim // TILE
+    up_arrived(0)
+    corner_lift(0)
+    block = pl.ds(0, cap)
+    remote(result.at[block], back.at[block], ret_go.at[0], ret_come.at[0], mate).wait_recv()
+    lax.fori_loop(0, tiles, combine_near, 0)
+    for u in range(1, half // TILE):
+        up_arrived(u)
+        corner_lift(u)
+
     def mate_copy(t):
         return remote(
             corner_out.at[:, tile_of(t)],
@@ -814,33 +835,19 @@
 
     def corner_drop(t):
         cols = tile_of(t)
-        for block, target, base in ((1, corner_out, 0), (0, back, cap)):
-            target[base : base + cap, cols] = jnp.dot(
-                corner_act[block * cap : (block + 1) * cap, :],
-                corner_down[:, cols],
-                preferred_element_type=f32,
-            ).astype(bf16)
-            if block == 1:
-                mate_copy(t).start()
-
-    def combine_near(t, carry):
-        cols = tile_of(t)
-        found = jnp.dot(pick_near[...], back[0:cap, cols], preferred_element_type=f32)
-        total[:, cols] = total[:, cols] + found
-        return carry
+        found = halves_dot(corner_act[...], corner_down[:, cols]).astype(bf16)
+        corner_out[:, cols] = found[cap:]
+        mate_copy(t).start()
+        back[cap : 2 * cap, cols] = found[:cap]
 
     def combine_rest(t):
         cols = tile_of(t)
         mate_copy(t).wait_recv()
         block = back.at[pl.ds(3 * cap, cap), cols]
         remote(block, block, late_go.at[0], late_come.at[t], mate).wait_recv()
-        found = jnp.dot(pick_rest[...], back[cap:, cols], preferred_element_type=f32)
+        found = halves_dot(pick_rest[...], back[cap:, cols])
         out_ref[:, cols] = (total[:, cols] + found).astype(bf16)
 
-    tiles = model_dim // TILE
-    block = pl.ds(0, cap)
-    remote(result.at[block], back.at[block], ret_go.at[0], ret_come.at[0], mate).wait_recv()
-    lax.fori_loop(0, tiles, combine_near, 0)
     for t in range(tiles):
         arrived(8 + t)
         corner_drop(t)
@@ -955,7 +962,7 @@
             dma((2,)),
             dma((12,)),
             dma((3, 2)),
-            dma((2, 5)),
+            dma((2, 6)),
             dma((12,)),
             dma((1,)),
             dma((2,)),

time: 64.7 us -> 64.1 us (level)
  Pallas kernels: 63.6 us -> 62.7 us
    pallas_call x1, Pallas kernels: 63.6 us -> 62.7 us  [run_fused(): pl.pallas_call(functools.partial(fused_kernel, count, tp_count), out_shap...]
where the time goes in v4:
time: 64.1 us; the launch traced here: 63.7 us
  Pallas kernels  62.7 us (98%)
  local copies, waits for them, and re-layouts  0.97 us (2%)
    pallas_call x1, Pallas kernels, run_fused(): pl.pallas_call(functools.partial(fused_kernel, count, tp_count), out_shap...  62.7 us

profile of v4, /device:TPU:0, one launch (start us, length us, event | category | flops | bytes accessed | tf_op | source)
XLA Modules:
  0.0 63.7 jit_solution(1702102616413623433)
XLA Ops:
  0.0 62.7 %shard_map.118 = bf16[512,1024]{1,0:T(8,128)(2,1)S(1)} custom-call(bf16[64,4096]{1,0:T(8,128)(2,1)} %bitcast.5, s32[1,4096]{1,0:T(1,128)} %bitcast.6, s32[2,512]{1,0:T(2,128)} %bitcast.7, f32[2,512]{1,0:T(2,128)} %bitcast.8, f32[1,1024]{1,0:T(1,128)} %bitcast.9, bf16[512,1024]{1,0:T(8,128)(2,1)} %gate_hbm.1, bf16[512,1024]{1,0:T(8,128)(2,1)} %resid_hbm.1, ...), custom_call_target="tpu_custom_call" | custom-call | flops 8053063680 | bytes 6291456 | tf_op jit(solution)/shard_map/pallas_call | solution.py:916
  62.7 1.0 %copy.14 = bf16[512,1024]{1,0:T(8,128)(2,1)} copy(bf16[512,1024]{1,0:T(8,128)(2,1)S(1)} %shard_map.118) | data formatting | bytes 2097152

commit v5 on v4

--- a/solution.py
+++ b/solution.py
@@ -420,6 +420,8 @@
     ]
 
     pieces = [(m, q) for q in range(4) for m in range(2)] + [(2, q) for q in range(4)]
+    groups = [range(0, 1), range(1, 4)] + [range(i, i + 2) for i in range(4, 12, 2)]
+    group_of = [g for g, some in enumerate(groups) for _ in some]
     sources = (w_gate, w_lift, w_down)
     far = partner(sp, 3, count)
 
@@ -453,7 +455,7 @@
             src,
             place(m, q, start, size),
             part_go.at[m // 2],
-            direct_come.at[i],
+            direct_come.at[group_of[i]],
             {"sp": far},
         )
 
@@ -464,58 +466,49 @@
             place(m, q, start, size),
             place(m, q, start, size),
             share_go.at[way, m // 2],
-            middle_come.at[i] if way == 1 else near_come.at[way // 2, i // 4 if i < 8 else i - 6],
+            middle_come.at[i // 8] if way == 1 else near_come.at[i // 4 if i < 8 else i - 6],
             {"tp": partner(tp, 6 if way == 1 else 2, tp_count)},
         )
 
-    def pass_on(i):
+    def bytes_of(some, zones):
+        size = sum(span(*pieces[i], zone)[1] for i in some for zone in zones)
+        if size > model_dim:
+            return corner_up.at[0, pl.ds(0, size // 2), :]
+        return corner_up.at[0, pl.ds(0, size), tile_of(0)]
+
+    def take(some, zones, sem):
+        ref = bytes_of(some, zones)
+        remote(ref, ref, share_go.at[0, 0], sem, mate).wait_recv()
+
+    def pass_on(g):
         @pl.when(at_end)
         def _():
-            fetch(i, 0).wait_recv()
-            share(i, 0, 0).start()
+            take(groups[g], (0,), direct_come.at[g])
+            for i in groups[g]:
+                share(i, 0, 0).start()
 
         @pl.when(inside)
         def _():
-            fetch(i, plane).wait_recv()
-            share(i, plane, 1).start()
-            share(i, plane, 0).start()
-
-    def relay(i):
+            take(groups[g], (1,), direct_come.at[g])
+            for i in groups[g]:
+                share(i, plane, 1).start()
+                share(i, plane, 0).start()
+
+    def relay(some):
         @pl.when(inside)
         def _():
-            share(i, 3 - plane, 1).wait_recv()
-            share(i, 3 - plane, 2).start()
-
-    def whole(zone, down):
-        start, size = span(2 if down else 0, 0, zone)
-        if down:
-            return corner_down.at[pl.ds(start, size), :]
-        size = sum(span(0, q, zone)[1] for q in range(2))
-        return corner_up.at[:, pl.ds(start, size), :]
-
-    def up_arrived(u):
-        def wait_for(zone, kind):
-            ref = whole(zone, False).at[:, :, tile_of(u)]
-            remote(ref, ref, share_go.at[0, 0], near_come.at[kind, u], mate).wait_recv()
-
+            take(some, (1,), middle_come.at[some[0] // 8])
+            for i in some:
+                share(i, 3 - plane, 2).start()
+
+    def arrived(some, k):
         @pl.when(at_end)
         def _():
-            wait_for(1, 0)
-            wait_for(2, 1)
+            take(some, (1, 2), near_come.at[k])
 
         @pl.when(inside)
         def _():
-            wait_for(0, 0)
-
-    def arrived(i):
-        @pl.when(at_end)
-        def _():
-            share(i, 1, 0).wait_recv()
-            share(i, 2, 2).wait_recv()
-
-        @pl.when(inside)
-        def _():
-            share(i, 0, 0).wait_recv()
+            take(some, (0,), near_come.at[k])
 
     def fetch_all(some):
         @pl.when(at_end)
@@ -575,7 +568,7 @@
         pool_copy(j).start()
 
     def pool_step(i, carry):
-        j = tp_count - 1 - i
+        j = lax.rem(i + 1, tp_count - 1) + 1
 
         @pl.when(j != tp)
         def _():
@@ -646,8 +639,7 @@
     found = found + weighed(late, 1, 0) + weighed(late, 2, 0)
     pick_rest[...] = found.astype(bf16)
 
-    for i in range(1, 4):
-        pass_on(i)
+    pass_on(1)
 
     for load in loads[7:]:
         load.wait()
@@ -679,8 +671,7 @@
         normed[block, :] = (x * scale * gain[...]).astype(bf16)
         return carry
 
-    for i in range(4, 6):
-        pass_on(i)
+    pass_on(2)
     lax.fori_loop(0, rows // 64, norm, 0)
 
     def pack_near(t, carry):
@@ -723,8 +714,6 @@
     for h, p in chunks:
         out_copy(h, p).start()
 
-    pass_on(6)
-
     def pack_local(t, carry):
         cols = tile_of(t)
         packed = halves_dot(onehot[1], normed[:, cols]).astype(bf16)
@@ -737,7 +726,7 @@
         corner.at[pl.ds(0, cap)], corner.at[pl.ds(cap, cap)], core_go.at[0], core_come.at[0], mate
     )
     corner_copy.start()
-    pass_on(7)
+    pass_on(3)
 
     def activate(gate, lift):
         gate = jnp.minimum(gate, 7.0)
@@ -765,8 +754,7 @@
         lax.fori_loop(0, model_dim // TILE, down, 0)
 
     ffn(own, local_out, 0)
-    pass_on(8)
-    pass_on(9)
+    pass_on(4)
 
     def combine_own(t, carry):
         cols = tile_of(t)
@@ -775,10 +763,8 @@
         return carry
 
     lax.fori_loop(0, model_dim // TILE, combine_own, 0)
-    pass_on(10)
-    pass_on(11)
-    for i in range(8):
-        relay(i)
+    pass_on(5)
+    relay(range(8))
 
     def near_arrived(h):
         block = pl.ds(h * cap, cap)
@@ -788,8 +774,7 @@
     ffn(recv, result, 0)
     for p in range(2):
         back_copy(p).start()
-    for i in range(8, 12):
-        relay(i)
+    relay(range(8, 12))
     near_arrived(1)
 
     def send_back(t):
@@ -815,13 +800,13 @@
         return carry
 
     tiles = model_dim // TILE
-    up_arrived(0)
+    arrived(range(4), 0)
     corner_lift(0)
     block = pl.ds(0, cap)
     remote(result.at[block], back.at[block], ret_go.at[0], ret_come.at[0], mate).wait_recv()
     lax.fori_loop(0, tiles, combine_near, 0)
     for u in range(1, half // TILE):
-        up_arrived(u)
+        arrived(range(4 * u, 4 * u + 4), u)
         corner_lift(u)
 
     def mate_copy(t):
@@ -849,7 +834,7 @@
         out_ref[:, cols] = (total[:, cols] + found).astype(bf16)
 
     for t in range(tiles):
-        arrived(8 + t)
+        arrived(range(8 + t, 9 + t), 2 + t)
         corner_drop(t)
         if t > 0:
             combine_rest(t - 1)
@@ -868,22 +853,21 @@
     remote(result.at[block], back.at[block], late_go.at[0], late_come.at[0], mate).wait_send()
     remote(corner_out, corner_out, mate_go.at[0], mate_come.at[0], mate).wait_send()
 
-    def gone(ref, sem):
-        remote(ref, ref, sem, direct_come.at[0], mate).wait_send()
+    def gone(zone, sems):
+        for k, some in enumerate((range(8), range(8, 12))):
+            ref = bytes_of(some, (zone,))
+            remote(ref, ref, sems.at[k], direct_come.at[0], mate).wait_send()
 
     @pl.when(at_end)
     def _():
-        for k in range(2):
-            gone(whole(0, k), part_go.at[k])
-            gone(whole(0, k), share_go.at[0, k])
+        gone(0, part_go)
+        gone(0, share_go.at[0])
 
     @pl.when(inside)
     def _():
-        for k in range(2):
-            gone(whole(plane, k), part_go.at[k])
-            gone(whole(plane, k), share_go.at[0, k])
-            gone(whole(plane, k), share_go.at[1, k])
-            gone(whole(3 - plane, k), share_go.at[2, k])
+        gone(1, part_go)
+        for way in range(3):
+            gone(1, share_go.at[way])
 
 
 def run_fused(
@@ -960,10 +944,10 @@
             dma((1,)),
             dma((1,)),
             dma((2,)),
-            dma((12,)),
+            dma((6,)),
             dma((3, 2)),
-            dma((2, 6)),
-            dma((12,)),
+            dma((6,)),
+            dma((2,)),
             dma((1,)),
             dma((2,)),
             dma((1,)),

time: 64.1 us -> 63.9 us (level)
  no operation moved by 1% of the time
where the time goes in v5:
time: 63.9 us; the launch traced here: 63.6 us
  Pallas kernels  62.6 us (98%)
  local copies, waits for them, and re-layouts  0.97 us (2%)
    pallas_call x1, Pallas kernels, run_fused(): pl.pallas_call(functools.partial(fused_kernel, count, tp_count), out_shap...  62.6 us

profile of v5, /device:TPU:0, one launch (start us, length us, event | category | flops | bytes accessed | tf_op | source)
XLA Modules:
  0.0 63.6 jit_solution(16583971700200574193)
XLA Ops:
  0.0 62.6 %shard_map.118 = bf16[512,1024]{1,0:T(8,128)(2,1)S(1)} custom-call(bf16[64,4096]{1,0:T(8,128)(2,1)} %bitcast.5, s32[1,4096]{1,0:T(1,128)} %bitcast.6, s32[2,512]{1,0:T(2,128)} %bitcast.7, f32[2,512]{1,0:T(2,128)} %bitcast.8, f32[1,1024]{1,0:T(1,128)} %bitcast.9, bf16[512,1024]{1,0:T(8,128)(2,1)} %gate_hbm.1, bf16[512,1024]{1,0:T(8,128)(2,1)} %resid_hbm.1, ...), custom_call_target="tpu_custom_call" | custom-call | flops 8053063680 | bytes 6291456 | tf_op jit(solution)/shard_map/pallas_call | solution.py:900
  62.6 1.0 %copy.14 = bf16[512,1024]{1,0:T(8,128)(2,1)} copy(bf16[512,1024]{1,0:T(8,128)(2,1)S(1)} %shard_map.118) | data formatting | bytes 2097152

commit v6 on v5

--- a/solution.py
+++ b/solution.py
@@ -377,24 +377,15 @@
             )
         )
     ]
+    barrier = pltpu.get_barrier_semaphore()
+
+    for axis, me, size in (("tp", tp, tp_count), ("sp", sp, count)):
+        for j in range(size - 1, 0, -1):
+            pl.semaphore_signal(
+                barrier, inc=1, device_id={axis: partner(me, j, size)}, device_id_type=MESH
+            )
     for load in loads[:5]:
         load.start()
-    barrier = pltpu.get_barrier_semaphore()
-
-    def greet_sp(j, carry):
-        pl.semaphore_signal(
-            barrier, inc=1, device_id={"sp": partner(sp, j, count)}, device_id_type=MESH
-        )
-        return carry
-
-    def greet_tp(j, carry):
-        pl.semaphore_signal(
-            barrier, inc=1, device_id={"tp": partner(tp, j, tp_count)}, device_id_type=MESH
-        )
-        return carry
-
-    lax.fori_loop(1, count, greet_sp, 0)
-    lax.fori_loop(1, tp_count, greet_tp, 0)
     def remote(src, dst, go, come, device):
         return pltpu.make_async_remote_copy(
             src_ref=src,

time: 63.9 us -> 63.9 us (level)
  no operation moved by 1% of the time
where the time goes in v6:
time: 63.9 us; the launch traced here: 63.6 us
  Pallas kernels  62.6 us (98%)
  local copies, waits for them, and re-layouts  0.97 us (2%)
    pallas_call x1, Pallas kernels, run_fused(): pl.pallas_call(functools.partial(fused_kernel, count, tp_count), out_shap...  62.6 us

profile of v6, /device:TPU:0, one launch (start us, length us, event | category | flops | bytes accessed | tf_op | source)
XLA Modules:
  0.0 63.6 jit_solution(4245775966786120966)
XLA Ops:
  0.0 62.6 %shard_map.118 = bf16[512,1024]{1,0:T(8,128)(2,1)S(1)} custom-call(bf16[64,4096]{1,0:T(8,128)(2,1)} %bitcast.5, s32[1,4096]{1,0:T(1,128)} %bitcast.6, s32[2,512]{1,0:T(2,128)} %bitcast.7, f32[2,512]{1,0:T(2,128)} %bitcast.8, f32[1,1024]{1,0:T(1,128)} %bitcast.9, bf16[512,1024]{1,0:T(8,128)(2,1)} %gate_hbm.1, bf16[512,1024]{1,0:T(8,128)(2,1)} %resid_hbm.1, ...), custom_call_target="tpu_custom_call" | custom-call | flops 8053063680 | bytes 6291456 | tf_op jit(solution)/shard_map/pallas_call | solution.py:891
  62.6 1.0 %copy.14 = bf16[512,1024]{1,0:T(8,128)(2,1)} copy(bf16[512,1024]{1,0:T(8,128)(2,1)S(1)} %shard_map.118) | data formatting | bytes 2097152
